TPU v7x, 32 devices: a whole 2x2x4 slice. The times are simulated.
32 devices in a mesh: sp: 16 (over z, y, x), tp: 2 (over core).
Axes of the slice: x: 2, y: 2, z: 4, core: 2. Of those that a mesh axis runs over, the one named last changes fastest.
Arguments:
- tokens: bfloat16 [4096, 2048], P('sp', 'tp'), may hold values from -6 to 6
- outer_gate: bfloat16 [2048, 1024], P(None, 'tp'), may hold values from -0.125 to 0.125
- inner_gate: bfloat16 [2048, 1024], P(None, 'tp'), may hold values from -0.125 to 0.125
- conv_input: bfloat16 [2048, 1024], P(None, 'tp'), may hold values from -0.125 to 0.125
- conv_taps: bfloat16 [3, 1024], P(None, 'tp'), may hold values from -3.5 to 3.5
- query_down: bfloat16 [2048, 512], P(None, 'tp'), may hold values from -0.125 to 0.125
- latent_down: bfloat16 [2048, 256], P(None, 'tp'), may hold values from -0.125 to 0.125
- rotary_down: bfloat16 [2048, 32], replicated, may hold values from -5.303301 to 5.303301
- query_gain: float32 [512], replicated, may hold values from 0.1 to 1.9
- latent_gain: float32 [256], replicated, may hold values from 0.1 to 1.9
- query_up: bfloat16 [512, 1536], P(None, 'tp'), may hold values from -0.52734375 to 0.52734375
- latent_up: bfloat16 [256, 2048], P(None, 'tp'), may hold values from -0.75 to 0.75
- conv_project: bfloat16 [1024, 2048], P('tp'), may hold values from -0.1875 to 0.1875
- attend_project: bfloat16 [1024, 2048], P('tp'), may hold values from -0.1875 to 0.1875
Outputs:
- mixed: bfloat16 [4096, 2048], P(('sp', 'tp'))
All inputs are finite; a program needn't handle non-finite values.
Results may differ from a plain program's by a relative error of at most 0.035.
Values may be sent and summed in bfloat16 or wider, within the bound.
A program may use at most 128 MiB of HBM per device.

v0:
```python
import jax
import numpy as np
import jax.numpy as jnp
from jax import lax
from jax.experimental import pallas as pl
from jax.experimental.pallas import tpu as pltpu
from jax.sharding import PartitionSpec as P

NOPE = 64
ROPE = 32
VDIM = 64
LANES = 128
ONES = 16
EDGE = 16

MESH = pl.DeviceIdType.MESH
neg_fill = -1e30
rotary_base = 10000.0
norm_epsilon = 1e-06
log2e = 1.4426950408889634


def dot(a, b, dims=((1,), (0,))):
    return lax.dot_general(a, b, (dims, ((), ())), preferred_element_type=jnp.float32)


def attend(lat, rot, qx_ref, up_ref, wvt_ref, best_ref, acc_ref, masked):
    heads = qx_ref.shape[0]
    expanded = dot(lat, up_ref[...]).astype(jnp.bfloat16)
    turned = dot(wvt_ref[...], lat, ((1,), (1,))).astype(jnp.bfloat16)
    ones = jnp.ones((ONES, lat.shape[0]), jnp.bfloat16)
    width = NOPE + VDIM
    for h in range(heads):
        key = jnp.concatenate([expanded[:, h * width : (h + 1) * width], rot], 1)
        s = dot(key, qx_ref[h])
        if masked:
            k_at = lax.broadcasted_iota(jnp.int32, s.shape, 0)
            q_at = lax.broadcasted_iota(jnp.int32, s.shape, 1)
            s = jnp.where(k_at <= q_at, s, neg_fill)
        values = jnp.concatenate([turned[h * VDIM : (h + 1) * VDIM], ones], 0)
        top = jnp.max(s, 0, keepdims=True)
        if masked:
            weight = jnp.exp2((s - top).astype(jnp.bfloat16))
            acc_ref[h] = dot(values, weight)
            best_ref[h] = top
        else:
            old = best_ref[h]
            new = jnp.maximum(old, top)
            weight = jnp.exp2((s - new).astype(jnp.bfloat16))
            acc_ref[h] = acc_ref[h] * jnp.exp2(old - new) + dot(values, weight)
            best_ref[h] = new


def mix_kernel(
    tok, inv_ref, taps_ref, qgain_ref, lgain_ref,
    ldown_in, qdown_in, rdown_in, inner_in, signal_in, outer_in, qup_in, up_in, cproj_in, aproj_in,
    out_ref,
    ldown, qdown, rdown, inner_w, signal_w, outer_w, qup, up_ref, cproj_ref, aproj_ref,
    xbuf, raw_lat, raw_query, edge, rim, padded, conv_ref, wvt_ref, qx_ref,
    lat, rot, best_ref, acc_ref, att, part_buf, in_buf,
    load_sem, front_send, front_recv, lat_send, lat_recv, rot_send, rot_recv, share_send, share_recv, tail_send, tail_recv,
):
    me = lax.axis_index("sp")
    t = lax.axis_index("tp")
    total = lax.axis_size("sp")
    ways = lax.axis_size("tp")
    planes = total // 4
    z = me // 4
    b0 = me % 2
    b1 = (me // 2) % 2
    a0 = 1 - t % 2
    rows = qx_ref.shape[2]
    short = rows // ways

    def block_of(plane, ka, kb):
        f0 = a0 * ka + (1 - a0) * kb
        f1 = a0 * kb + (1 - a0) * ka
        return plane * 4 + (b1 + f1 * (1 - 2 * b1)) * 2 + b0 + f0 * (1 - 2 * b0)

    up = lax.rem(me + 4, total)
    down = lax.rem(me + total - 4, total)
    after = lax.rem(me + 1, total)
    before = lax.rem(me + total - 1, total)
    a_peer = block_of(z, 1, 0)
    b_peer = block_of(z, 0, 1)
    mates = [lax.rem(t + o, ways) for o in range(1, ways)]

    barrier = pltpu.get_barrier_semaphore()
    for target in [(up, t), (down, t), (a_peer, t), (b_peer, t), (after, t), (before, t)] + [(me, mate) for mate in mates]:
        pl.semaphore_signal(barrier, inc=1, device_id=target, device_id_type=MESH)

    pairs = (
        (ldown_in, ldown), (qdown_in, qdown), (rdown_in, rdown), (inner_in, inner_w), (signal_in, signal_w),
        (outer_in, outer_w), (qup_in, qup), (up_in, up_ref), (cproj_in, cproj_ref), (aproj_in, aproj_ref),
    )
    loads = [pltpu.make_async_copy(a, b, load_sem.at[i]) for i, (a, b) in enumerate(pairs)]
    for copy in loads:
        copy.start()
    pl.semaphore_wait(barrier, 6 + len(mates))

    def to_mates(source, slots, kind):
        return [
            pltpu.make_async_remote_copy(
                source, slots.at[o], front_send.at[kind, o], front_recv.at[kind, o],
                device_id=(me, mate), device_id_type=MESH,
            )
            for o, mate in enumerate(mates)
        ]

    token_sends = to_mates(tok, xbuf, 0)
    for copy in token_sends:
        copy.start()
    depth = tok.shape[1]

    def rows_from(weight, o):
        at = pl.multiple_of(lax.rem(t + ways - o, ways) * depth, depth)
        if weight is rdown:
            return weight[:, pl.ds(at, depth)]
        return weight[pl.ds(at, depth), :]

    def project(x, weight, o):
        return dot(x, rows_from(weight, o), ((1,), (1 if weight is rdown else 0,)))

    def rest(value, weight):
        for o in range(1, ways):
            value = value + project(xbuf[o - 1], weight, o)
        return value

    for copy in loads[:3]:
        copy.wait()
    first = [project(tok[...], weight, 0) for weight in (ldown, qdown, rdown)]
    for copy in token_sends:
        copy.wait_recv()
    lat_part, query_part, turn_part = [rest(v, w) for v, w in zip(first, (ldown, qdown, rdown))]
    raw_lat[ways - 1] = lat_part.astype(jnp.bfloat16)
    raw_query[ways - 1] = query_part.astype(jnp.bfloat16)
    latent_sends = to_mates(raw_lat.at[ways - 1], raw_lat, 1) + to_mates(raw_query.at[ways - 1], raw_query, 2)
    for copy in latent_sends:
        copy.start()

    position = (me * rows + lax.broadcasted_iota(jnp.int32, (1, rows), 1)).astype(jnp.float32)
    angle = inv_ref[...] * position
    cosine = jnp.cos(angle)
    sine = jnp.sin(angle)
    half = ROPE // 2

    def rotated(values):
        a = values[:half]
        b = values[half:]
        return jnp.concatenate([a * cosine - b * sine, a * sine + b * cosine], 0).astype(jnp.bfloat16)

    turn = jnp.concatenate([turn_part, jnp.zeros((rows, LANES - ROPE), jnp.float32)], 1).T
    rot[me] = rotated(turn[:ROPE])

    loads[3].wait()
    loads[4].wait()
    inner = rest(dot(tok[...], rows_from(inner_w, 0)), inner_w)
    signal = rest(dot(tok[...], rows_from(signal_w, 0)), signal_w)
    gated = (inner * signal).astype(jnp.bfloat16)
    padded[EDGE:] = gated.astype(jnp.float32)
    edge[...] = gated[rows - EDGE :]

    def whole(raw, gain_ref):
        values = jnp.concatenate([raw[lax.rem(t + ways - 1 - s, ways)] for s in range(ways)], 1).astype(jnp.float32)
        factor = lax.rsqrt(jnp.mean(values * values, -1, keepdims=True) + norm_epsilon)
        return (values * factor * gain_ref[...]).astype(jnp.bfloat16)

    for copy in latent_sends:
        copy.wait_recv()
    latent_norm = whole(raw_lat, lgain_ref)
    wide = latent_norm.shape[1] // ways
    for s in range(ways):
        lat[me, s] = latent_norm[:, s * wide : (s + 1) * wide]

    def hop(j, k, target):
        return [
            pltpu.make_async_remote_copy(
                buf.at[j, t] if split else buf.at[j],
                buf.at[j, t] if split else buf.at[j],
                send.at[j, k],
                recv.at[j],
                device_id=(target, t),
                device_id_type=MESH,
            )
            for buf, send, recv, split in ((lat, lat_send, lat_recv, True), (rot, rot_send, rot_recv, False))
        ]

    def start(j, k, target):
        for copy in hop(j, k, target):
            copy.start()

    def arrive(j):
        for copy in hop(j, 0, up):
            copy.wait_recv()

    def shares(j):
        return [
            pltpu.make_async_remote_copy(
                lat.at[j, t],
                lat.at[j, t],
                share_send.at[j, o],
                share_recv.at[j, o],
                device_id=(me, mate),
                device_id_type=MESH,
            )
            for o, mate in enumerate(mates)
        ]

    def share_landed(j):
        for o in range(len(mates)):
            source = lax.rem(t + ways - 1 - o, ways)
            pltpu.make_async_remote_copy(
                lat.at[j, source],
                lat.at[j, source],
                share_send.at[j, o],
                share_recv.at[j, o],
                device_id=(me, mates[o]),
                device_id_type=MESH,
            ).wait_recv()

    def share(j):
        @pl.when(j < me)
        def _():
            for copy in shares(j):
                copy.start()

    def spread(j):
        @pl.when(z + 1 < planes)
        def _():
            start(j, 0, up)

        start(j, 1, a_peer)
        start(j, 2, b_peer)

    def stage_a(d):
        j = block_of(z - d, 0, 0)
        arrive(j)
        spread(j)
        share(j)

    def stage_b(d):
        j = block_of(z - d, 1, 0)
        arrive(j)
        start(j, 2, b_peer)
        share(j)

    def stage_c(d):
        for ka in (0, 1):
            j = block_of(z - d, ka, 1)
            arrive(j)
            share(j)

    def block(j, masked):
        latent = jnp.concatenate([lat[j, s] for s in range(ways)], 1)
        turned = rot[j].astype(jnp.float32)
        turned = jnp.concatenate([turned, jnp.zeros((LANES - ROPE, rows), jnp.float32)], 0)
        turned = turned.T.astype(jnp.bfloat16)
        attend(latent, turned, qx_ref, up_ref, wvt_ref, best_ref, acc_ref, masked)

    spread(me)
    rim_copy = pltpu.make_async_remote_copy(
        edge, rim, front_send.at[3, 0], front_recv.at[3, 0], device_id=(after, t), device_id_type=MESH
    )

    @pl.when(me + 1 < total)
    def _():
        rim_copy.start()

    loads[6].wait()
    loads[7].wait()
    scale = (NOPE + ROPE) ** (-0.5) * log2e
    query = (dot(whole(raw_query, qgain_ref), qup[...]) * scale).T
    heads = qx_ref.shape[0]
    size = NOPE + ROPE
    turned_up = up_ref[...].astype(jnp.float32).T.astype(jnp.bfloat16)
    for h in range(heads):
        base = h * size
        qx_ref[h, :NOPE] = query[base : base + NOPE].astype(jnp.bfloat16)
        qx_ref[h, NOPE : NOPE + VDIM] = jnp.zeros((VDIM, rows), jnp.bfloat16)
        qx_ref[h, NOPE + VDIM : NOPE + VDIM + ROPE] = rotated(query[base + NOPE : base + size])
        qx_ref[h, NOPE + VDIM + ROPE :] = jnp.zeros((LANES - ROPE, rows), jnp.bfloat16)
        low = h * (NOPE + VDIM) + NOPE
        wvt_ref[h * VDIM : (h + 1) * VDIM] = turned_up[low : low + VDIM]

    block(me, True)
    stage_b(0)
    loads[5].wait()
    outer = rest(dot(tok[...], rows_from(outer_w, 0)), outer_w)

    @pl.when(me > 0)
    def _():
        rim_copy.wait_recv()
        padded[:EDGE] = rim[...].astype(jnp.float32)

    @pl.when(me == 0)
    def _():
        padded[:EDGE] = jnp.zeros((EDGE, padded.shape[1]), jnp.float32)

    reach = taps_ref.shape[0] - 1
    taps = taps_ref[...].astype(jnp.float32)
    filtered = padded[EDGE:] * taps[reach : reach + 1, :]
    for k in range(reach):
        filtered = filtered + padded[EDGE - reach + k : EDGE - reach + k + rows] * taps[k : k + 1, :]
    conv_ref[...] = (outer * filtered).astype(jnp.bfloat16)
    stage_c(0)

    @pl.loop(0, 4 * (z + 1))
    def _(n):
        d = n // 4
        k = n % 4
        for order, stage in enumerate((stage_a, stage_b, stage_c)):

            @pl.when(jnp.logical_and(k == order, d < z))
            def _():
                stage(d + 1)

        j = block_of(z - d, k % 2, k // 2)

        @pl.when(j < me)
        def _():
            share_landed(j)
            block(j, False)

    for h in range(qx_ref.shape[0]):
        acc = acc_ref[h]
        acc_ref[h, :VDIM] = acc[:VDIM] / acc[VDIM : VDIM + 1]
    flat = jnp.concatenate([acc_ref[h, :VDIM] for h in range(qx_ref.shape[0])], 0)
    att[...] = flat.T.astype(jnp.bfloat16)

    loads[8].wait()
    loads[9].wait()

    def part(owner):
        at = pl.ds(pl.multiple_of(owner * short, short), short)
        return (dot(conv_ref[at, :], cproj_ref[...]) + dot(att[at, :], aproj_ref[...])).astype(jnp.bfloat16)

    tails = []
    for o, mate in enumerate(mates):
        part_buf[o] = part(mate)
        tails.append(
            pltpu.make_async_remote_copy(
                part_buf.at[o],
                in_buf.at[o],
                tail_send.at[o],
                tail_recv.at[o],
                device_id=(me, mate),
                device_id_type=MESH,
            )
        )
        tails[-1].start()
    result = part(t).astype(jnp.float32)
    for o, copy in enumerate(tails):
        copy.wait_recv()
        result = result + in_buf[o].astype(jnp.float32)
    out_ref[...] = result.astype(jnp.bfloat16)
    for copy in tails + token_sends + latent_sends:
        copy.wait_send()

    @pl.when(me + 1 < total)
    def _():
        rim_copy.wait_send()

    @pl.loop(0, z + 1)
    def _(d):
        def sent(j, k):
            for copy in hop(j, k, up):
                copy.wait_send()

        mine = block_of(z - d, 0, 0)

        @pl.when(z + 1 < planes)
        def _():
            sent(mine, 0)

        sent(mine, 1)
        sent(mine, 2)
        sent(block_of(z - d, 1, 0), 2)
        for k in range(4):
            j = block_of(z - d, k % 2, k // 2)

            @pl.when(j < me)
            def _():
                for copy in shares(j):
                    copy.wait_send()


def local(
    tokens,
    outer_gate,
    inner_gate,
    conv_input,
    conv_taps,
    query_down,
    latent_down,
    rotary_down,
    query_gain,
    latent_gain,
    query_up,
    latent_up,
    conv_project,
    attend_project,
):
    rows = tokens.shape[0]
    heads = query_up.shape[1] // (NOPE + ROPE)
    ways = lax.axis_size("tp")
    blocks = lax.axis_size("sp")
    model = conv_project.shape[1]
    kvr = latent_up.shape[0]
    channels = conv_project.shape[0]
    half = ROPE // 2
    inverse = jnp.asarray(np.float32(rotary_base) ** (-(np.arange(half, dtype=np.float32) * 2.0 / (2 * half))), jnp.float32)
    vmem = pl.BlockSpec(memory_space=pltpu.VMEM)
    dma = pltpu.SemaphoreType.DMA
    mates = ways - 1
    big = (
        latent_down, query_down, rotary_down.T, inner_gate, conv_input,
        outer_gate, query_up, latent_up, conv_project, attend_project,
    )

    def half_type(*shape):
        return pltpu.VMEM(shape, jnp.bfloat16)

    def full_type(*shape):
        return pltpu.VMEM(shape, jnp.float32)

    return pl.pallas_call(
        mix_kernel,
        out_shape=jax.ShapeDtypeStruct((rows // ways, model), jnp.bfloat16),
        in_specs=[vmem] * 5 + [pl.BlockSpec(memory_space=pl.ANY)] * len(big),
        out_specs=vmem,
        scratch_shapes=[half_type(*array.shape) for array in big]
        + [
            half_type(mates, *tokens.shape),
            half_type(ways, rows, latent_down.shape[1]),
            half_type(ways, rows, query_down.shape[1]),
            half_type(EDGE, channels),
            half_type(EDGE, channels),
            full_type(EDGE + rows, channels),
            half_type(rows, channels),
            half_type(heads * VDIM, kvr),
            half_type(heads, NOPE + VDIM + LANES, rows),
            half_type(blocks, ways, rows, kvr // ways),
            half_type(blocks, ROPE, rows),
            full_type(heads, 1, rows),
            full_type(heads, VDIM + ONES, rows),
            half_type(rows, heads * VDIM),
            half_type(mates, rows // ways, model),
            half_type(mates, rows // ways, model),
            dma((len(big),)),
            dma((4, mates)),
            dma((4, mates)),
            dma((blocks, 3)),
            dma((blocks,)),
            dma((blocks, 3)),
            dma((blocks,)),
            dma((blocks, mates)),
            dma((blocks, mates)),
            dma((mates,)),
            dma((mates,)),
        ],
        compiler_params=pltpu.CompilerParams(
            vmem_limit_bytes=60 * 1024 * 1024, collective_id=0, has_side_effects=True
        ),
    )(
        tokens,
        inverse[:, None],
        conv_taps,
        query_gain[None, :],
        latent_gain[None, :],
        *big,
    )


def solution(mesh):
    split = P(None, "tp")
    in_specs = (P("sp", "tp"),) + (split,) * 6 + (P(),) * 3 + (split,) * 2 + (P("tp", None),) * 2
    out_specs = P(("sp", "tp"), None)
    return jax.shard_map(local, mesh=mesh, in_specs=in_specs, out_specs=out_specs, check_vma=False)
```

profile of v0, /device:TPU:25, one launch (start us, length us, event | category | flops | bytes accessed | tf_op | source)
XLA Modules:
  0.0 69.3 jit_solution(17236011099774139375)
XLA Ops:
  0.0 67.4 %shard_map.145 = bf16[128,2048]{1,0:T(8,128)(2,1)} custom-call(bf16[256,1024]{1,0:T(8,128)(2,1)} %tok.1, f32[16,1]{1,0:T(8,128)} %constant.3.inv_ref, bf16[3,512]{1,0:T(4,128)(2,1)} %taps_ref.1, f32[1,512]{1,0:T(1,128)} %bitcast.4, f32[1,256]{1,0:T(1,128)} %bitcast.5, bf16[2048,128]{1,0:T(8,128)(2,1)} %ldown_in.1, bf16[2048,256]{1,0:T(8,128)(2,1)} %qdown_in.1, ...), custom_call_target="tpu_custom_call" | custom-call | tf_op jit(solution)/shard_map/pallas_call | solution.py:426
  67.4 1.9 %copy.17 = bf16[128,2048]{1,0:T(8,128)(2,1)} copy(bf16[128,2048]{1,0:T(8,128)(2,1)} %shard_map.145) | data formatting | bytes 1048576
where the time goes:
time: 69.7 us; the launch traced here: 69.3 us
  Pallas kernels  67.4 us (97%)
  local copies, waits for them, and re-layouts  1.88 us (3%)
    pallas_call x1, Pallas kernels, local(): pl.pallas_call(mix_kernel, out_shape=jax.ShapeDtypeStruct((rows // ways,...  67.4 us
    unnamed x1, local copies, waits for them, and re-layouts  1.88 us

commit v1 on v0

v1 whole, which is shorter than its diff:
```python
import jax
import numpy as np
import jax.numpy as jnp
from jax import lax
from jax.experimental import pallas as pl
from jax.experimental.pallas import tpu as pltpu
from jax.sharding import PartitionSpec as P

NOPE = 64
ROPE = 32
VDIM = 64
LANES = 128
ONES = 16
EDGE = 16
RING = 8
LAG = 2

MESH = pl.DeviceIdType.MESH
neg_fill = -1e30
rotary_base = 10000.0
norm_epsilon = 1e-06
log2e = 1.4426950408889634


def dot(a, b, dims=((1,), (0,))):
    return lax.dot_general(a, b, (dims, ((), ())), preferred_element_type=jnp.float32)


def unit(lat_parts, rot_parts, qx_ref, wk_ref, wvt_ref, keys, turned, scores, weights, best_ref, acc_ref, masked):
    heads, _, rows = qx_ref.shape
    latent = jnp.concatenate(lat_parts, 0)
    rot = jnp.concatenate(rot_parts, 0)
    span = latent.shape[0]
    keys[:span] = dot(latent, wk_ref[...]).astype(jnp.bfloat16)
    flat = dot(wvt_ref[...], latent, ((1,), (1,))).astype(jnp.bfloat16)
    for h in range(heads):
        turned[h, :VDIM, :span] = flat[h * VDIM : (h + 1) * VDIM]
    ring = scores.shape[0]
    tops = [None] * heads

    def score(h):
        pair = h // 2 * 2 * NOPE
        key = jnp.concatenate([keys[:span, pair : pair + 2 * NOPE], rot], 1)
        s = dot(key, qx_ref[h])
        if masked:
            k_at = lax.broadcasted_iota(jnp.int32, s.shape, 0)
            q_at = lax.broadcasted_iota(jnp.int32, s.shape, 1)
            s = jnp.where(k_at <= q_at, s, neg_fill)
        scores[h % ring, :span] = s
        top = jnp.max(s, 0, keepdims=True)
        if masked:
            tops[h] = (top, None)
        else:
            old = best_ref[h]
            top = jnp.maximum(old, top)
            tops[h] = (top, jnp.exp2(old - top))
        best_ref[h] = top

    def soften(h):
        weights[h % ring, :span] = jnp.exp2((scores[h % ring, :span] - tops[h][0]).astype(jnp.bfloat16))

    def gather(h):
        fresh = dot(turned[h, :, :span], weights[h % ring, :span])
        acc_ref[h] = fresh if masked else acc_ref[h] * tops[h][1] + fresh

    for step in range(heads + 2 * LAG):
        if step < heads:
            score(step)
        if 0 <= step - LAG < heads:
            soften(step - LAG)
        if 0 <= step - 2 * LAG < heads:
            gather(step - 2 * LAG)


def mix_kernel(
    tok_in, inv_ref, taps_ref, qgain_ref, lgain_ref,
    ldown_in, qdown_in, rdown_in, inner_in, signal_in, up_in, qup_in, outer_in, cproj_in, aproj_in,
    out_ref,
    tok, ldown, qdown, rdown, inner_w, signal_w, up_ref, qup, outer_w, cproj_ref, aproj_ref,
    xbuf, raw_lat, raw_query, edge, rim, padded, conv_ref, wk_ref, wvt_ref, qx_ref,
    kv, keys, turned, scores, weights, best_ref, acc_ref, att, early, cpart, part_buf, in_buf,
    load_sem, front_send, front_recv, up_send, side_send, kv_recv, share_send, share_recv, tail_send, tail_recv,
):
    me = lax.axis_index("sp")
    t = lax.axis_index("tp")
    total = lax.axis_size("sp")
    ways = lax.axis_size("tp")
    planes = total // 4
    z = me // 4
    b0 = me % 2
    b1 = (me // 2) % 2
    heads, _, rows = qx_ref.shape
    short = rows // ways
    cross = (1 - 2 * b0, 2 - 4 * b1, 3 - 2 * b0 - 4 * b1)
    after = lax.rem(me + 1, total)
    before = lax.rem(me + total - 1, total)
    mates = [lax.rem(t + o, ways) for o in range(1, ways)]

    barrier = pltpu.get_barrier_semaphore()
    targets = [(me, mate) for mate in mates] + [(me + c, t) for c in cross]
    targets += [(lax.rem(me + 4 * d, total), t) for d in range(1, planes)] + [(after, t), (before, t)]
    for target in targets:
        pl.semaphore_signal(barrier, inc=1, device_id=target, device_id_type=MESH)

    pairs = (
        (tok_in, tok), (ldown_in, ldown), (qdown_in, qdown), (rdown_in, rdown), (inner_in, inner_w), (signal_in, signal_w),
        (up_in, up_ref), (qup_in, qup), (outer_in, outer_w), (cproj_in, cproj_ref), (aproj_in, aproj_ref),
    )
    loads = [pltpu.make_async_copy(a, b, load_sem.at[i]) for i, (a, b) in enumerate(pairs)]
    for copy in loads:
        copy.start()

    position = (me * rows + lax.broadcasted_iota(jnp.int32, (1, rows), 1)).astype(jnp.float32)
    angle = inv_ref[...] * position
    cosine = jnp.cos(angle)
    sine = jnp.sin(angle)
    half = ROPE // 2

    def rotated(values):
        a = values[:half]
        b = values[half:]
        return jnp.concatenate([a * cosine - b * sine, a * sine + b * cosine], 0).astype(jnp.bfloat16)

    for h in range(heads):
        turned[h, VDIM:] = jnp.ones((ONES, turned.shape[2]), jnp.bfloat16)
    pl.semaphore_wait(barrier, len(targets))
    loads[0].wait()

    def to_mates(source, slots, kind):
        return [
            pltpu.make_async_remote_copy(
                source, slots.at[o], front_send.at[kind, o], front_recv.at[kind, o],
                device_id=(me, mate), device_id_type=MESH,
            )
            for o, mate in enumerate(mates)
        ]

    token_sends = to_mates(tok, xbuf, 0)
    for copy in token_sends:
        copy.start()
    depth = tok.shape[1]

    def rows_from(weight, o):
        at = pl.multiple_of(lax.rem(t + ways - o, ways) * depth, depth)
        if weight is rdown:
            return weight[:, pl.ds(at, depth)]
        return weight[pl.ds(at, depth), :]

    def project(x, weight, o):
        return dot(x, rows_from(weight, o), ((1,), (1 if weight is rdown else 0,)))

    def rest(value, weight):
        more = project(xbuf[0], weight, 1)
        for o in range(2, ways):
            more = more + project(xbuf[o - 1], weight, o)
        return value + more

    for copy in loads[1:4]:
        copy.wait()
    first = [project(tok[...], weight, 0) for weight in (ldown, qdown, rdown)]
    wides = (inner_w, signal_w, outer_w)
    for i in range(2):
        loads[4 + i].wait()
        early[i] = project(tok[...], wides[i], 0)
    for copy in token_sends:
        copy.wait_recv()
    lat_part, query_part, turn_part = [rest(v, w) for v, w in zip(first, (ldown, qdown, rdown))]
    raw_lat[ways - 1] = lat_part.astype(jnp.bfloat16)
    raw_query[ways - 1] = query_part.astype(jnp.bfloat16)
    latent_sends = to_mates(raw_lat.at[ways - 1], raw_lat, 1) + to_mates(raw_query.at[ways - 1], raw_query, 2)
    for copy in latent_sends:
        copy.start()

    turn = jnp.concatenate([turn_part, jnp.zeros((rows, LANES - ROPE), jnp.float32)], 1).T
    spun = rotated(turn[:ROPE])

    inner = rest(early[0], inner_w)
    signal = rest(early[1], signal_w)
    gated = (inner * signal).astype(jnp.bfloat16)
    padded[EDGE:] = gated.astype(jnp.float32)
    edge[...] = gated[rows - EDGE :]

    def whole(raw, gain_ref):
        values = jnp.concatenate([raw[lax.rem(t + ways - 1 - s, ways)] for s in range(ways)], 1).astype(jnp.float32)
        factor = lax.rsqrt(jnp.mean(values * values, -1, keepdims=True) + norm_epsilon)
        return (values * factor * gain_ref[...]).astype(jnp.bfloat16)

    for copy in latent_sends[: len(mates)]:
        copy.wait_recv()
    latent_norm = whole(raw_lat, lgain_ref)
    wide = kv.shape[3]
    for s in range(ways):
        kv[me, s, :rows] = latent_norm[:, s * wide : (s + 1) * wide]
        kv[me, s, rows:] = spun[:, s * wide : (s + 1) * wide]

    def send(j, target, sem):
        return pltpu.make_async_remote_copy(
            kv.at[j, t], kv.at[j, t], sem, kv_recv.at[j], device_id=(target, t), device_id_type=MESH
        )

    def shares(j):
        return [
            pltpu.make_async_remote_copy(
                kv.at[j, t], kv.at[j, t], share_send.at[j, o], share_recv.at[j, o],
                device_id=(me, mate), device_id_type=MESH,
            )
            for o, mate in enumerate(mates)
        ]

    def landed(j):
        for o in range(len(mates)):
            source = lax.rem(t + ways - 1 - o, ways)
            pltpu.make_async_remote_copy(
                kv.at[j, source], kv.at[j, source], share_send.at[j, o], share_recv.at[j, o],
                device_id=(me, mates[o]), device_id_type=MESH,
            ).wait_recv()

    def collect(j):
        send(j, me, side_send.at[j, 0]).wait_recv()
        for copy in shares(j):
            copy.start()

    def relay(j):
        collect(j)
        for k in range(3):
            send(j, me + cross[k], side_send.at[j, k]).start()

    def own_sends(go):
        for d in range(1, planes):

            @pl.when(z + d < planes)
            def _():
                go(send(me, me + 4 * d, up_send.at[d - 1]))

        for k, bit in enumerate((b0, b1, b1)):

            @pl.when(bit == 0)
            def _():
                go(send(me, me + cross[k], side_send.at[me, k]))

    own_sends(lambda copy: copy.start())
    rim_copy = pltpu.make_async_remote_copy(
        edge, rim, front_send.at[3, 0], front_recv.at[3, 0], device_id=(after, t), device_id_type=MESH
    )

    @pl.when(me + 1 < total)
    def _():
        rim_copy.start()

    loads[6].wait()
    low = lax.broadcasted_iota(jnp.int32, (1, 2 * NOPE), 1) < NOPE
    width = NOPE + VDIM
    for p in range(heads // 2):
        even = up_ref[:, 2 * p * width : (2 * p + 1) * width].astype(jnp.float32)
        odd = up_ref[:, (2 * p + 1) * width : (2 * p + 2) * width].astype(jnp.float32)
        at = slice(p * width, (p + 1) * width)
        wk_ref[:, at] = jnp.where(low, even, pltpu.roll(odd, NOPE, 1)).astype(jnp.bfloat16)
        wvt_ref[at] = jnp.where(low, pltpu.roll(even, NOPE, 1), odd).T.astype(jnp.bfloat16)

    loads[7].wait()
    for copy in latent_sends[len(mates) :]:
        copy.wait_recv()
    scale = (NOPE + ROPE) ** (-0.5) * log2e
    query = (dot(whole(raw_query, qgain_ref), qup[...]) * scale).T
    size = NOPE + ROPE
    for h in range(heads):
        base = h * size
        side = h % 2 * NOPE
        qx_ref[h, side : side + NOPE] = query[base : base + NOPE].astype(jnp.bfloat16)
        qx_ref[h, NOPE - side : 2 * NOPE - side] = jnp.zeros((NOPE, rows), jnp.bfloat16)
        qx_ref[h, 2 * NOPE : 2 * NOPE + ROPE] = rotated(query[base + NOPE : base + size])
        qx_ref[h, 2 * NOPE + ROPE :] = jnp.zeros((LANES - ROPE, rows), jnp.bfloat16)

    def run(blocks, masked):
        lat_parts = []
        rot_parts = []
        for j in blocks:
            lat_parts.append(jnp.concatenate([kv[j, s, :rows] for s in range(ways)], 1))
            spin = jnp.concatenate([kv[j, s, rows:] for s in range(ways)], 1).astype(jnp.float32)
            spin = jnp.concatenate([spin, jnp.zeros((LANES - ROPE, rows), jnp.float32)], 0)
            rot_parts.append(spin.T.astype(jnp.bfloat16))
        unit(
            lat_parts, rot_parts, qx_ref, wk_ref, wvt_ref, keys, turned, scores, weights, best_ref, acc_ref, masked
        )

    run([me], True)
    loads[8].wait()
    outer = rest(project(tok[...], outer_w, 0), outer_w)

    @pl.when(me > 0)
    def _():
        rim_copy.wait_recv()
        padded[:EDGE] = rim[...].astype(jnp.float32)

    @pl.when(me == 0)
    def _():
        padded[:EDGE] = jnp.zeros((EDGE, padded.shape[1]), jnp.float32)

    reach = taps_ref.shape[0] - 1
    taps = taps_ref[...].astype(jnp.float32)
    filtered = padded[EDGE:] * taps[reach : reach + 1, :]
    for k in range(reach):
        filtered = filtered + padded[EDGE - reach + k : EDGE - reach + k + rows] * taps[k : k + 1, :]
    conv_ref[...] = (outer * filtered).astype(jnp.bfloat16)

    @pl.when(b0 == 1)
    def _():
        collect(me + cross[0])

    @pl.when(z > 0)
    def _():
        relay(me - 4)

    loads[9].wait()
    cpart[...] = dot(conv_ref[...], cproj_ref[...])

    @pl.when(b0 == 1)
    def _():
        landed(me + cross[0])
        run([me + cross[0]], False)

    @pl.when(b1 == 1)
    def _():
        collect(me + cross[1])
        collect(me + cross[2])

    @pl.loop(0, 2 * z + 1)
    def _(n):
        plane = (n + 1) // 2
        odd = n % 2
        own = me - 4 * plane

        @pl.when(n + 2 <= z)
        def _():
            relay(own + 4 * plane - 4 * (n + 2))

        @pl.when(n < 2 * z)
        def _():
            then = me - 4 * ((n + 2) // 2)

            @pl.when(odd == 0)
            def _():
                collect(then + cross[0])

            @pl.when(odd == 1)
            def _():
                collect(then + cross[1])
                collect(then + cross[2])

        left = own + (1 - odd) * cross[1]
        right = own + odd * cross[0] + (1 - odd) * cross[2]

        @pl.when(n + b1 > 0)
        def _():
            landed(left)
            landed(right)
            run([left, right], False)

    for h in range(heads):
        acc = acc_ref[h]
        acc_ref[h, :VDIM] = acc[:VDIM] / acc[VDIM : VDIM + 1]
    flat = jnp.concatenate([acc_ref[h, :VDIM] for h in range(heads)], 0)
    att[...] = flat.T.astype(jnp.bfloat16)

    loads[10].wait()

    def part(owner):
        at = pl.ds(pl.multiple_of(owner * short, short), short)
        return (cpart[at, :] + dot(att[at, :], aproj_ref[...])).astype(jnp.bfloat16)

    tails = []
    for o, mate in enumerate(mates):
        part_buf[o] = part(mate)
        tails.append(
            pltpu.make_async_remote_copy(
                part_buf.at[o], in_buf.at[o], tail_send.at[o], tail_recv.at[o],
                device_id=(me, mate), device_id_type=MESH,
            )
        )
        tails[-1].start()
    result = part(t).astype(jnp.float32)
    for o, copy in enumerate(tails):
        copy.wait_recv()
        result = result + in_buf[o].astype(jnp.float32)
    out_ref[...] = result.astype(jnp.bfloat16)
    for copy in tails + token_sends + latent_sends:
        copy.wait_send()

    @pl.when(me + 1 < total)
    def _():
        rim_copy.wait_send()

    own_sends(lambda copy: copy.wait_send())

    @pl.when(b0 == 1)
    def _():
        for copy in shares(me + cross[0]):
            copy.wait_send()

    @pl.when(b1 == 1)
    def _():
        for copy in shares(me + cross[1]) + shares(me + cross[2]):
            copy.wait_send()

    @pl.loop(1, z + 1)
    def _(d):
        j = me - 4 * d
        for k in range(3):
            send(j, me + cross[k], side_send.at[j, k]).wait_send()
        for c in (0,) + cross:
            for copy in shares(j + c):
                copy.wait_send()


def local(
    tokens,
    outer_gate,
    inner_gate,
    conv_input,
    conv_taps,
    query_down,
    latent_down,
    rotary_down,
    query_gain,
    latent_gain,
    query_up,
    latent_up,
    conv_project,
    attend_project,
):
    rows = tokens.shape[0]
    heads = query_up.shape[1] // (NOPE + ROPE)
    ways = lax.axis_size("tp")
    blocks = lax.axis_size("sp")
    model = conv_project.shape[1]
    kvr = latent_up.shape[0]
    channels = conv_project.shape[0]
    half = ROPE // 2
    inverse = jnp.asarray(np.float32(rotary_base) ** (-(np.arange(half, dtype=np.float32) * 2.0 / (2 * half))), jnp.float32)
    vmem = pl.BlockSpec(memory_space=pltpu.VMEM)
    dma = pltpu.SemaphoreType.DMA
    mates = ways - 1
    ring = min(heads, RING)
    big = (
        tokens, latent_down, query_down, rotary_down.T, inner_gate, conv_input,
        latent_up, query_up, outer_gate, conv_project, attend_project,
    )

    def half_type(*shape):
        return pltpu.VMEM(shape, jnp.bfloat16)

    def full_type(*shape):
        return pltpu.VMEM(shape, jnp.float32)

    return pl.pallas_call(
        mix_kernel,
        out_shape=jax.ShapeDtypeStruct((rows // ways, model), jnp.bfloat16),
        in_specs=[pl.BlockSpec(memory_space=pl.ANY)] + [vmem] * 4 + [pl.BlockSpec(memory_space=pl.ANY)] * (len(big) - 1),
        out_specs=vmem,
        scratch_shapes=[half_type(*array.shape) for array in big]
        + [
            half_type(mates, *tokens.shape),
            half_type(ways, rows, latent_down.shape[1]),
            half_type(ways, rows, query_down.shape[1]),
            half_type(EDGE, channels),
            half_type(EDGE, channels),
            full_type(EDGE + rows, channels),
            half_type(rows, channels),
            half_type(kvr, heads * NOPE),
            half_type(heads * VDIM, kvr),
            half_type(heads, 2 * NOPE + LANES, rows),
            half_type(blocks, ways, rows + ROPE, kvr // ways),
            half_type(2 * rows, heads * NOPE),
            half_type(heads, VDIM + ONES, 2 * rows),
            full_type(ring, 2 * rows, rows),
            half_type(ring, 2 * rows, rows),
            full_type(heads, 1, rows),
            full_type(heads, VDIM + ONES, rows),
            half_type(rows, heads * VDIM),
            full_type(2, rows, channels),
            full_type(rows, model),
            half_type(mates, rows // ways, model),
            half_type(mates, rows // ways, model),
            dma((len(big),)),
            dma((4, mates)),
            dma((4, mates)),
            dma((blocks // 4 - 1,)),
            dma((blocks, 3)),
            dma((blocks,)),
            dma((blocks, mates)),
            dma((blocks, mates)),
            dma((mates,)),
            dma((mates,)),
        ],
        compiler_params=pltpu.CompilerParams(
            vmem_limit_bytes=60 * 1024 * 1024, collective_id=0, has_side_effects=True
        ),
    )(
        tokens,
        inverse[:, None],
        conv_taps,
        query_gain[None, :],
        latent_gain[None, :],
        *big[1:],
    )


def solution(mesh):
    split = P(None, "tp")
    in_specs = (P("sp", "tp"),) + (split,) * 6 + (P(),) * 3 + (split,) * 2 + (P("tp", None),) * 2
    out_specs = P(("sp", "tp"), None)
    return jax.shard_map(local, mesh=mesh, in_specs=in_specs, out_specs=out_specs, check_vma=False)
```

time: 69.7 us -> 36.7 us (0.53)
  the two profiles are of different devices: /device:TPU:25 before, /device:TPU:23 now
where the time goes in v1:
time: 36.7 us; the launch traced here: 36.5 us
  Pallas kernels  34.6 us (94%)
  local copies, waits for them, and re-layouts  1.88 us (5%)
    pallas_call x1, Pallas kernels, local(): pl.pallas_call(mix_kernel, out_shape=jax.ShapeDtypeStruct((rows // ways,...  34.6 us
    unnamed x1, local copies, waits for them, and re-layouts  1.88 us

profile of v1, /device:TPU:23, one launch (start us, length us, event | category | flops | bytes accessed | tf_op | source)
XLA Modules:
  0.0 36.5 jit_solution(16823115032902914491)
XLA Ops:
  0.0 34.6 %shard_map.145 = bf16[128,2048]{1,0:T(8,128)(2,1)} custom-call(bf16[256,1024]{1,0:T(8,128)(2,1)} %tok_in.1, f32[16,1]{1,0:T(8,128)} %constant.3.inv_ref, bf16[3,512]{1,0:T(4,128)(2,1)} %taps_ref.1, f32[1,512]{1,0:T(1,128)} %bitcast.4, f32[1,256]{1,0:T(1,128)} %bitcast.5, bf16[2048,128]{1,0:T(8,128)(2,1)} %ldown_in.1, bf16[2048,256]{1,0:T(8,128)(2,1)} %qdown_in.1, ...), custom_call_target="tpu_custom_call" | custom-call | tf_op jit(solution)/shard_map/pallas_call | solution.py:455
  34.6 1.9 %copy.17 = bf16[128,2048]{1,0:T(8,128)(2,1)} copy(bf16[128,2048]{1,0:T(8,128)(2,1)} %shard_map.145) | data formatting | bytes 1048576

commit v2 on v1

--- a/solution.py
+++ b/solution.py
@@ -14,6 +14,7 @@
 EDGE = 16
 RING = 8
 LAG = 2
+EAGER = 9
 
 MESH = pl.DeviceIdType.MESH
 neg_fill = -1e30
@@ -73,12 +74,11 @@
 
 
 def mix_kernel(
-    tok_in, inv_ref, taps_ref, qgain_ref, lgain_ref,
-    ldown_in, qdown_in, rdown_in, inner_in, signal_in, up_in, qup_in, outer_in, cproj_in, aproj_in,
+    inv_in, tok_in, ldown_in, rdown_in, qdown_in, up_in, inner_in, signal_in, lgain_in, qgain_in, qup_in, taps_in, outer_in, cproj_in, aproj_in,
     out_ref,
-    tok, ldown, qdown, rdown, inner_w, signal_w, up_ref, qup, outer_w, cproj_ref, aproj_ref,
+    inv_ref, tok, ldown, rdown, qdown, up_ref, inner_w, signal_w, lgain_ref, qgain_ref, qup, taps_ref, outer_w, cproj_ref, aproj_ref,
     xbuf, raw_lat, raw_query, edge, rim, padded, conv_ref, wk_ref, wvt_ref, qx_ref,
-    kv, keys, turned, scores, weights, best_ref, acc_ref, att, early, cpart, part_buf, in_buf,
+    kv, keys, turned, scores, weights, best_ref, acc_ref, att, small, held, cpart, part_buf, in_buf,
     load_sem, front_send, front_recv, up_send, side_send, kv_recv, share_send, share_recv, tail_send, tail_recv,
 ):
     me = lax.axis_index("sp")
@@ -103,26 +103,14 @@
         pl.semaphore_signal(barrier, inc=1, device_id=target, device_id_type=MESH)
 
     pairs = (
-        (tok_in, tok), (ldown_in, ldown), (qdown_in, qdown), (rdown_in, rdown), (inner_in, inner_w), (signal_in, signal_w),
-        (up_in, up_ref), (qup_in, qup), (outer_in, outer_w), (cproj_in, cproj_ref), (aproj_in, aproj_ref),
+        (tok_in, tok), (ldown_in, ldown), (rdown_in, rdown), (qdown_in, qdown), (inv_in, inv_ref),
+        (lgain_in, lgain_ref), (qgain_in, qgain_ref), (taps_in, taps_ref), (inner_in, inner_w), (up_in, up_ref),
+        (qup_in, qup), (signal_in, signal_w), (outer_in, outer_w), (cproj_in, cproj_ref), (aproj_in, aproj_ref),
     )
     loads = [pltpu.make_async_copy(a, b, load_sem.at[i]) for i, (a, b) in enumerate(pairs)]
-    for copy in loads:
+    for copy in loads[:EAGER]:
         copy.start()
 
-    position = (me * rows + lax.broadcasted_iota(jnp.int32, (1, rows), 1)).astype(jnp.float32)
-    angle = inv_ref[...] * position
-    cosine = jnp.cos(angle)
-    sine = jnp.sin(angle)
-    half = ROPE // 2
-
-    def rotated(values):
-        a = values[:half]
-        b = values[half:]
-        return jnp.concatenate([a * cosine - b * sine, a * sine + b * cosine], 0).astype(jnp.bfloat16)
-
-    for h in range(heads):
-        turned[h, VDIM:] = jnp.ones((ONES, turned.shape[2]), jnp.bfloat16)
     pl.semaphore_wait(barrier, len(targets))
     loads[0].wait()
 
@@ -138,6 +126,20 @@
     token_sends = to_mates(tok, xbuf, 0)
     for copy in token_sends:
         copy.start()
+    loads[4].wait()
+    position = (me * rows + lax.broadcasted_iota(jnp.int32, (1, rows), 1)).astype(jnp.float32)
+    angle = inv_ref[...] * position
+    cosine = jnp.cos(angle)
+    sine = jnp.sin(angle)
+    half = ROPE // 2
+
+    def rotated(values):
+        a = values[:half]
+        b = values[half:]
+        return jnp.concatenate([a * cosine - b * sine, a * sine + b * cosine], 0).astype(jnp.bfloat16)
+
+    for h in range(heads):
+        turned[h, VDIM:] = jnp.ones((ONES, turned.shape[2]), jnp.bfloat16)
     depth = tok.shape[1]
 
     def rows_from(weight, o):
@@ -157,36 +159,40 @@
 
     for copy in loads[1:4]:
         copy.wait()
-    first = [project(tok[...], weight, 0) for weight in (ldown, qdown, rdown)]
-    wides = (inner_w, signal_w, outer_w)
-    for i in range(2):
-        loads[4 + i].wait()
-        early[i] = project(tok[...], wides[i], 0)
+    for copy in loads[EAGER:]:
+        copy.start()
+    narrow = (ldown, qdown, rdown)
+    spots = []
+    for weight in narrow:
+        start = spots[-1].stop if spots else 0
+        spots.append(slice(start, start + (LANES if weight is rdown else weight.shape[1])))
+    for weight, spot in zip(narrow, spots):
+        small[:, spot.start : spot.start + (ROPE if weight is rdown else weight.shape[1])] = project(tok[...], weight, 0)
     for copy in token_sends:
         copy.wait_recv()
-    lat_part, query_part, turn_part = [rest(v, w) for v, w in zip(first, (ldown, qdown, rdown))]
-    raw_lat[ways - 1] = lat_part.astype(jnp.bfloat16)
-    raw_query[ways - 1] = query_part.astype(jnp.bfloat16)
-    latent_sends = to_mates(raw_lat.at[ways - 1], raw_lat, 1) + to_mates(raw_query.at[ways - 1], raw_query, 2)
+    raw_lat[ways - 1] = rest(small[:, spots[0]], ldown).astype(jnp.bfloat16)
+    latent_sends = to_mates(raw_lat.at[ways - 1], raw_lat, 1)
+    query_sends = to_mates(raw_query.at[ways - 1], raw_query, 2)
     for copy in latent_sends:
         copy.start()
-
+    raw_query[ways - 1] = rest(small[:, spots[1]], qdown).astype(jnp.bfloat16)
+    for copy in query_sends:
+        copy.start()
+    turn_part = rest(small[:, spots[2].start : spots[2].start + ROPE], rdown)
     turn = jnp.concatenate([turn_part, jnp.zeros((rows, LANES - ROPE), jnp.float32)], 1).T
     spun = rotated(turn[:ROPE])
 
-    inner = rest(early[0], inner_w)
-    signal = rest(early[1], signal_w)
-    gated = (inner * signal).astype(jnp.bfloat16)
-    padded[EDGE:] = gated.astype(jnp.float32)
-    edge[...] = gated[rows - EDGE :]
+    loads[8].wait()
+    held[...] = rest(project(tok[...], inner_w, 0), inner_w)
 
     def whole(raw, gain_ref):
         values = jnp.concatenate([raw[lax.rem(t + ways - 1 - s, ways)] for s in range(ways)], 1).astype(jnp.float32)
         factor = lax.rsqrt(jnp.mean(values * values, -1, keepdims=True) + norm_epsilon)
         return (values * factor * gain_ref[...]).astype(jnp.bfloat16)
 
-    for copy in latent_sends[: len(mates)]:
+    for copy in latent_sends:
         copy.wait_recv()
+    loads[5].wait()
     latent_norm = whole(raw_lat, lgain_ref)
     wide = kv.shape[3]
     for s in range(ways):
@@ -220,18 +226,28 @@
         for copy in shares(j):
             copy.start()
 
-    def relay(j):
-        collect(j)
+    def lift(d, go):
+        j = me - 4 * d
+
+        @pl.when(jnp.logical_and(d % 3 < 2, z + 1 < planes))
+        def _():
+            go(send(j, me + 4, up_send.at[j, 0]))
+
+        @pl.when(jnp.logical_and(d % 3 == 0, z + 3 < planes))
+        def _():
+            go(send(j, me + 12, up_send.at[j, 1]))
+
+    def relay(d):
+        j = me - 4 * d
+        send(j, me, side_send.at[j, 0]).wait_recv()
+        lift(d, lambda copy: copy.start())
         for k in range(3):
             send(j, me + cross[k], side_send.at[j, k]).start()
+        for copy in shares(j):
+            copy.start()
 
     def own_sends(go):
-        for d in range(1, planes):
-
-            @pl.when(z + d < planes)
-            def _():
-                go(send(me, me + 4 * d, up_send.at[d - 1]))
-
+        lift(0, go)
         for k, bit in enumerate((b0, b1, b1)):
 
             @pl.when(bit == 0)
@@ -239,15 +255,7 @@
                 go(send(me, me + cross[k], side_send.at[me, k]))
 
     own_sends(lambda copy: copy.start())
-    rim_copy = pltpu.make_async_remote_copy(
-        edge, rim, front_send.at[3, 0], front_recv.at[3, 0], device_id=(after, t), device_id_type=MESH
-    )
-
-    @pl.when(me + 1 < total)
-    def _():
-        rim_copy.start()
-
-    loads[6].wait()
+    loads[9].wait()
     low = lax.broadcasted_iota(jnp.int32, (1, 2 * NOPE), 1) < NOPE
     width = NOPE + VDIM
     for p in range(heads // 2):
@@ -257,8 +265,9 @@
         wk_ref[:, at] = jnp.where(low, even, pltpu.roll(odd, NOPE, 1)).astype(jnp.bfloat16)
         wvt_ref[at] = jnp.where(low, pltpu.roll(even, NOPE, 1), odd).T.astype(jnp.bfloat16)
 
-    loads[7].wait()
-    for copy in latent_sends[len(mates) :]:
+    loads[6].wait()
+    loads[10].wait()
+    for copy in query_sends:
         copy.wait_recv()
     scale = (NOPE + ROPE) ** (-0.5) * log2e
     query = (dot(whole(raw_query, qgain_ref), qup[...]) * scale).T
@@ -284,8 +293,38 @@
         )
 
     run([me], True)
-    loads[8].wait()
-    outer = rest(project(tok[...], outer_w, 0), outer_w)
+    loads[11].wait()
+    signal = rest(project(tok[...], signal_w, 0), signal_w)
+    gated = (held[...] * signal).astype(jnp.bfloat16)
+    padded[EDGE:] = gated.astype(jnp.float32)
+    edge[...] = gated[rows - EDGE :]
+    rim_copy = pltpu.make_async_remote_copy(
+        edge, rim, front_send.at[3, 0], front_recv.at[3, 0], device_id=(after, t), device_id_type=MESH
+    )
+
+    @pl.when(me + 1 < total)
+    def _():
+        rim_copy.start()
+
+    loads[12].wait()
+    held[...] = rest(project(tok[...], outer_w, 0), outer_w)
+
+    @pl.when(z > 0)
+    def _():
+        relay(1)
+
+    @pl.when(b0 == 1)
+    def _():
+        collect(me + cross[0])
+        landed(me + cross[0])
+        run([me + cross[0]], False)
+
+    @pl.when(b1 == 1)
+    def _():
+        collect(me + cross[1])
+        collect(me + cross[2])
+
+    loads[7].wait()
 
     @pl.when(me > 0)
     def _():
@@ -301,28 +340,10 @@
     filtered = padded[EDGE:] * taps[reach : reach + 1, :]
     for k in range(reach):
         filtered = filtered + padded[EDGE - reach + k : EDGE - reach + k + rows] * taps[k : k + 1, :]
-    conv_ref[...] = (outer * filtered).astype(jnp.bfloat16)
-
-    @pl.when(b0 == 1)
-    def _():
-        collect(me + cross[0])
-
-    @pl.when(z > 0)
-    def _():
-        relay(me - 4)
-
-    loads[9].wait()
+    conv_ref[...] = (held[...] * filtered).astype(jnp.bfloat16)
+
+    loads[13].wait()
     cpart[...] = dot(conv_ref[...], cproj_ref[...])
-
-    @pl.when(b0 == 1)
-    def _():
-        landed(me + cross[0])
-        run([me + cross[0]], False)
-
-    @pl.when(b1 == 1)
-    def _():
-        collect(me + cross[1])
-        collect(me + cross[2])
 
     @pl.loop(0, 2 * z + 1)
     def _(n):
@@ -332,7 +353,7 @@
 
         @pl.when(n + 2 <= z)
         def _():
-            relay(own + 4 * plane - 4 * (n + 2))
+            relay(n + 2)
 
         @pl.when(n < 2 * z)
         def _():
@@ -362,7 +383,7 @@
     flat = jnp.concatenate([acc_ref[h, :VDIM] for h in range(heads)], 0)
     att[...] = flat.T.astype(jnp.bfloat16)
 
-    loads[10].wait()
+    loads[14].wait()
 
     def part(owner):
         at = pl.ds(pl.multiple_of(owner * short, short), short)
@@ -383,7 +404,7 @@
         copy.wait_recv()
         result = result + in_buf[o].astype(jnp.float32)
     out_ref[...] = result.astype(jnp.bfloat16)
-    for copy in tails + token_sends + latent_sends:
+    for copy in tails + token_sends + latent_sends + query_sends:
         copy.wait_send()
 
     @pl.when(me + 1 < total)
@@ -405,6 +426,7 @@
     @pl.loop(1, z + 1)
     def _(d):
         j = me - 4 * d
+        lift(d, lambda copy: copy.wait_send())
         for k in range(3):
             send(j, me + cross[k], side_send.at[j, k]).wait_send()
         for c in (0,) + cross:
@@ -442,8 +464,8 @@
     mates = ways - 1
     ring = min(heads, RING)
     big = (
-        tokens, latent_down, query_down, rotary_down.T, inner_gate, conv_input,
-        latent_up, query_up, outer_gate, conv_project, attend_project,
+        inverse[:, None], tokens, latent_down, rotary_down.T, query_down, latent_up, inner_gate, conv_input,
+        latent_gain[None, :], query_gain[None, :], query_up, conv_taps, outer_gate, conv_project, attend_project,
     )
 
     def half_type(*shape):
@@ -454,10 +476,10 @@
 
     return pl.pallas_call(
         mix_kernel,
-        out_shape=jax.ShapeDtypeStruct((rows // ways, model), jnp.bfloat16),
-        in_specs=[pl.BlockSpec(memory_space=pl.ANY)] + [vmem] * 4 + [pl.BlockSpec(memory_space=pl.ANY)] * (len(big) - 1),
+        out_shape=pltpu.VMEM((rows // ways, model), jnp.bfloat16),
+        in_specs=[pl.BlockSpec(memory_space=pl.ANY)] * len(big),
         out_specs=vmem,
-        scratch_shapes=[half_type(*array.shape) for array in big]
+        scratch_shapes=[pltpu.VMEM(array.shape, array.dtype) for array in big]
         + [
             half_type(mates, *tokens.shape),
             half_type(ways, rows, latent_down.shape[1]),
@@ -477,14 +499,15 @@
             full_type(heads, 1, rows),
             full_type(heads, VDIM + ONES, rows),
             half_type(rows, heads * VDIM),
-            full_type(2, rows, channels),
+            full_type(rows, latent_down.shape[1] + query_down.shape[1] + LANES),
+            full_type(rows, channels),
             full_type(rows, model),
             half_type(mates, rows // ways, model),
             half_type(mates, rows // ways, model),
             dma((len(big),)),
             dma((4, mates)),
             dma((4, mates)),
-            dma((blocks // 4 - 1,)),
+            dma((blocks, 2)),
             dma((blocks, 3)),
             dma((blocks,)),
             dma((blocks, mates)),
@@ -495,14 +518,7 @@
         compiler_params=pltpu.CompilerParams(
             vmem_limit_bytes=60 * 1024 * 1024, collective_id=0, has_side_effects=True
         ),
-    )(
-        tokens,
-        inverse[:, None],
-        conv_taps,
-        query_gain[None, :],
-        latent_gain[None, :],
-        *big[1:],
-    )
+    )(*big)
 
 
 def solution(mesh):

time: 36.7 us -> 33.3 us (0.907)
  the two profiles are of different devices: /device:TPU:23 before, /device:TPU:25 now
where the time goes in v2:
time: 33.3 us; the launch traced here: 33.1 us
  Pallas kernels  32.3 us (97%)
  local copies, waits for them, and re-layouts  0.8 us (2%)
    pallas_call x1, Pallas kernels, local(): pl.pallas_call(mix_kernel, out_shape=pltpu.VMEM((rows // ways, model), jn...  32.3 us
    unnamed x1, local copies, waits for them, and re-layouts  0.8 us

profile of v2, /device:TPU:25, one launch (start us, length us, event | category | flops | bytes accessed | tf_op | source)
XLA Modules:
  0.0 33.1 jit_solution(14049286784248313207)
XLA Ops:
  0.0 32.3 %shard_map.145 = bf16[128,2048]{1,0:T(8,128)(2,1)S(1)} custom-call(f32[16,1]{1,0:T(8,128)} %constant.3.inv_in, bf16[256,1024]{1,0:T(8,128)(2,1)} %tok_in.1, bf16[2048,128]{1,0:T(8,128)(2,1)} %ldown_in.1, bf16[32,2048]{1,0:T(8,128)(2,1)} %bitcast.3, bf16[2048,256]{1,0:T(8,128)(2,1)} %qdown_in.1, bf16[256,1024]{1,0:T(8,128)(2,1)} %up_in.1, ...), custom_call_target="tpu_custom_call" | custom-call | tf_op jit(solution)/shard_map/pallas_call | solution.py:477
  32.3 0.8 %copy.17 = bf16[128,2048]{1,0:T(8,128)(2,1)} copy(bf16[128,2048]{1,0:T(8,128)(2,1)S(1)} %shard_map.145) | data formatting | bytes 1048576

commit v3 on v2

--- a/solution.py
+++ b/solution.py
@@ -15,6 +15,7 @@
 RING = 8
 LAG = 2
 EAGER = 9
+CHUNKS = 2
 
 MESH = pl.DeviceIdType.MESH
 neg_fill = -1e30
@@ -182,8 +183,6 @@
     turn = jnp.concatenate([turn_part, jnp.zeros((rows, LANES - ROPE), jnp.float32)], 1).T
     spun = rotated(turn[:ROPE])
 
-    loads[8].wait()
-    held[...] = rest(project(tok[...], inner_w, 0), inner_w)
 
     def whole(raw, gain_ref):
         values = jnp.concatenate([raw[lax.rem(t + ways - 1 - s, ways)] for s in range(ways)], 1).astype(jnp.float32)
@@ -221,40 +220,49 @@
                 device_id=(me, mates[o]), device_id_type=MESH,
             ).wait_recv()
 
+    def arrive(j):
+        send(j, me, side_send.at[0, 0]).wait_recv()
+
     def collect(j):
-        send(j, me, side_send.at[j, 0]).wait_recv()
+        arrive(j)
         for copy in shares(j):
             copy.start()
 
-    def lift(d, go):
+    def lift(d, go, steps):
+        for step in steps:
+            starts = d % 4 == 0 if step > 1 else jnp.logical_or(d % 4 == 0, d % 4 == 3)
+
+            @pl.when(jnp.logical_and(starts, z + step < planes))
+            def _():
+                go(send(me - 4 * d, me + 4 * step, up_send.at[d, step - 1]))
+
+    def pass_on(d, ks):
+        for k in ks:
+            send(me - 4 * d, me + cross[k], side_send.at[d, k]).start()
+
+    def relay(d, ks=(0, 1, 2)):
         j = me - 4 * d
-
-        @pl.when(jnp.logical_and(d % 3 < 2, z + 1 < planes))
-        def _():
-            go(send(j, me + 4, up_send.at[j, 0]))
-
-        @pl.when(jnp.logical_and(d % 3 == 0, z + 3 < planes))
-        def _():
-            go(send(j, me + 12, up_send.at[j, 1]))
-
-    def relay(d):
-        j = me - 4 * d
-        send(j, me, side_send.at[j, 0]).wait_recv()
-        lift(d, lambda copy: copy.start())
-        for k in range(3):
-            send(j, me + cross[k], side_send.at[j, k]).start()
+        arrive(j)
+        lift(d, begin, (1, 2, 3))
+        pass_on(d, ks)
         for copy in shares(j):
             copy.start()
 
-    def own_sends(go):
-        lift(0, go)
-        for k, bit in enumerate((b0, b1, b1)):
-
-            @pl.when(bit == 0)
+    def begin(copy):
+        copy.start()
+
+    def finish(copy):
+        copy.wait_send()
+
+    def own_side(go, ks):
+        for k in ks:
+
+            @pl.when((b0, b1, b1)[k] == 0)
             def _():
-                go(send(me, me + cross[k], side_send.at[me, k]))
-
-    own_sends(lambda copy: copy.start())
+                go(send(me, me + cross[k], side_send.at[0, k]))
+
+    lift(0, begin, (1,))
+    own_side(begin, (0, 1))
     loads[9].wait()
     low = lax.broadcasted_iota(jnp.int32, (1, 2 * NOPE), 1) < NOPE
     width = NOPE + VDIM
@@ -292,10 +300,15 @@
             lat_parts, rot_parts, qx_ref, wk_ref, wvt_ref, keys, turned, scores, weights, best_ref, acc_ref, masked
         )
 
+    lift(0, begin, (2,))
+    own_side(begin, (2,))
     run([me], True)
+    lift(0, begin, (3,))
+    loads[8].wait()
+    inner = rest(project(tok[...], inner_w, 0), inner_w)
     loads[11].wait()
     signal = rest(project(tok[...], signal_w, 0), signal_w)
-    gated = (held[...] * signal).astype(jnp.bfloat16)
+    gated = (inner * signal).astype(jnp.bfloat16)
     padded[EDGE:] = gated.astype(jnp.float32)
     edge[...] = gated[rows - EDGE :]
     rim_copy = pltpu.make_async_remote_copy(
@@ -306,12 +319,17 @@
     def _():
         rim_copy.start()
 
+    @pl.when(z > 0)
+    def _():
+        relay(1, (0, 1))
+
     loads[12].wait()
     held[...] = rest(project(tok[...], outer_w, 0), outer_w)
 
     @pl.when(z > 0)
     def _():
-        relay(1)
+        pass_on(1, (2,))
+
 
     @pl.when(b0 == 1)
     def _():
@@ -324,26 +342,27 @@
         collect(me + cross[1])
         collect(me + cross[2])
 
-    loads[7].wait()
-
-    @pl.when(me > 0)
-    def _():
-        rim_copy.wait_recv()
-        padded[:EDGE] = rim[...].astype(jnp.float32)
-
-    @pl.when(me == 0)
-    def _():
-        padded[:EDGE] = jnp.zeros((EDGE, padded.shape[1]), jnp.float32)
-
-    reach = taps_ref.shape[0] - 1
-    taps = taps_ref[...].astype(jnp.float32)
-    filtered = padded[EDGE:] * taps[reach : reach + 1, :]
-    for k in range(reach):
-        filtered = filtered + padded[EDGE - reach + k : EDGE - reach + k + rows] * taps[k : k + 1, :]
-    conv_ref[...] = (held[...] * filtered).astype(jnp.bfloat16)
-
-    loads[13].wait()
-    cpart[...] = dot(conv_ref[...], cproj_ref[...])
+    def convolve():
+        loads[7].wait()
+
+        @pl.when(me > 0)
+        def _():
+            rim_copy.wait_recv()
+            padded[:EDGE] = rim[...].astype(jnp.float32)
+
+        @pl.when(me == 0)
+        def _():
+            padded[:EDGE] = jnp.zeros((EDGE, padded.shape[1]), jnp.float32)
+
+        reach = taps_ref.shape[0] - 1
+        taps = taps_ref[...].astype(jnp.float32)
+        filtered = padded[EDGE:] * taps[reach : reach + 1, :]
+        for k in range(reach):
+            filtered = filtered + padded[EDGE - reach + k : EDGE - reach + k + rows] * taps[k : k + 1, :]
+        conv_ref[...] = (held[...] * filtered).astype(jnp.bfloat16)
+
+        loads[13].wait()
+        cpart[...] = dot(conv_ref[...], cproj_ref[...])
 
     @pl.loop(0, 2 * z + 1)
     def _(n):
@@ -351,22 +370,33 @@
         odd = n % 2
         own = me - 4 * plane
 
-        @pl.when(n + 2 <= z)
-        def _():
-            relay(n + 2)
-
-        @pl.when(n < 2 * z)
-        def _():
+        def ahead(when):
             then = me - 4 * ((n + 2) // 2)
 
-            @pl.when(odd == 0)
+            @pl.when(jnp.logical_and(when, jnp.logical_and(n < 2 * z, odd == 0)))
             def _():
                 collect(then + cross[0])
 
-            @pl.when(odd == 1)
+            @pl.when(jnp.logical_and(when, jnp.logical_and(n < 2 * z, odd == 1)))
             def _():
                 collect(then + cross[1])
                 collect(then + cross[2])
+
+        @pl.when(jnp.logical_and(n == 0, b1 == 1))
+        def _():
+            convolve()
+
+        late = jnp.logical_and(n == 1, b1 == 0)
+        ahead(jnp.logical_not(late))
+        far = (n + b1) // 2 + 2
+
+        @pl.when(jnp.logical_and(jnp.logical_or(n == 0, (n + b1) % 2 == 0), far <= z))
+        def _():
+            relay(far)
+
+        @pl.when(jnp.logical_and(n == 0, b1 == 0))
+        def _():
+            convolve()
 
         left = own + (1 - odd) * cross[1]
         right = own + odd * cross[0] + (1 - odd) * cross[2]
@@ -377,33 +407,54 @@
             landed(right)
             run([left, right], False)
 
-    for h in range(heads):
-        acc = acc_ref[h]
-        acc_ref[h, :VDIM] = acc[:VDIM] / acc[VDIM : VDIM + 1]
-    flat = jnp.concatenate([acc_ref[h, :VDIM] for h in range(heads)], 0)
-    att[...] = flat.T.astype(jnp.bfloat16)
+        ahead(late)
 
     loads[14].wait()
 
-    def part(owner):
+    def settle(at):
+        flat = []
+        for h in range(heads):
+            acc = acc_ref[h, :, at]
+            flat.append(acc[:VDIM] / acc[VDIM : VDIM + 1])
+        return jnp.concatenate(flat, 0).T.astype(jnp.bfloat16)
+
+    if short % LANES:
+        att[...] = settle(slice(None))
+
+    model = cpart.shape[1]
+    step = model // CHUNKS
+
+    def rows_of(owner):
         at = pl.ds(pl.multiple_of(owner * short, short), short)
-        return (cpart[at, :] + dot(att[at, :], aproj_ref[...])).astype(jnp.bfloat16)
+        return at, (att[at, :] if short % LANES else settle(at))
+
+    def part(at, mixed, c):
+        cols = slice(c * step, (c + 1) * step)
+        return (cpart[at, cols] + dot(mixed, aproj_ref[:, cols])).astype(jnp.bfloat16)
 
     tails = []
     for o, mate in enumerate(mates):
-        part_buf[o] = part(mate)
-        tails.append(
-            pltpu.make_async_remote_copy(
-                part_buf.at[o], in_buf.at[o], tail_send.at[o], tail_recv.at[o],
-                device_id=(me, mate), device_id_type=MESH,
+        at, mixed = rows_of(mate)
+        for c in range(CHUNKS):
+            cols = pl.ds(c * step, step)
+            part_buf[o, :, cols] = part(at, mixed, c)
+            tails.append(
+                pltpu.make_async_remote_copy(
+                    part_buf.at[o, :, cols], in_buf.at[o, :, cols], tail_send.at[o, c], tail_recv.at[o, c],
+                    device_id=(me, mate), device_id_type=MESH,
+                )
             )
-        )
-        tails[-1].start()
-    result = part(t).astype(jnp.float32)
-    for o, copy in enumerate(tails):
-        copy.wait_recv()
-        result = result + in_buf[o].astype(jnp.float32)
-    out_ref[...] = result.astype(jnp.bfloat16)
+            tails[-1].start()
+    at, mixed = rows_of(t)
+    for c in range(CHUNKS):
+        cpart[:short, c * step : (c + 1) * step] = part(at, mixed, c).astype(jnp.float32)
+    for c in range(CHUNKS):
+        cols = slice(c * step, (c + 1) * step)
+        result = cpart[:short, cols]
+        for o in range(len(mates)):
+            tails[o * CHUNKS + c].wait_recv()
+            result = result + in_buf[o, :, cols].astype(jnp.float32)
+        out_ref[:, cols] = result.astype(jnp.bfloat16)
     for copy in tails + token_sends + latent_sends + query_sends:
         copy.wait_send()
 
@@ -411,7 +462,8 @@
     def _():
         rim_copy.wait_send()
 
-    own_sends(lambda copy: copy.wait_send())
+    lift(0, finish, (1, 2, 3))
+    own_side(finish, (0, 1, 2))
 
     @pl.when(b0 == 1)
     def _():
@@ -426,9 +478,9 @@
     @pl.loop(1, z + 1)
     def _(d):
         j = me - 4 * d
-        lift(d, lambda copy: copy.wait_send())
+        lift(d, finish, (1, 2, 3))
         for k in range(3):
-            send(j, me + cross[k], side_send.at[j, k]).wait_send()
+            send(j, me + cross[k], side_send.at[d, k]).wait_send()
         for c in (0,) + cross:
             for copy in shares(j + c):
                 copy.wait_send()
@@ -507,13 +559,13 @@
             dma((len(big),)),
             dma((4, mates)),
             dma((4, mates)),
-            dma((blocks, 2)),
-            dma((blocks, 3)),
+            dma((blocks // 4, 3)),
+            dma((blocks // 4, 3)),
             dma((blocks,)),
             dma((blocks, mates)),
             dma((blocks, mates)),
-            dma((mates,)),
-            dma((mates,)),
+            dma((mates, CHUNKS)),
+            dma((mates, CHUNKS)),
         ],
         compiler_params=pltpu.CompilerParams(
             vmem_limit_bytes=60 * 1024 * 1024, collective_id=0, has_side_effects=True

time: 33.3 us -> 32.7 us (0.982)
  Pallas kernels: 32.3 us -> 31.8 us
    pallas_call x1, Pallas kernels: 32.3 us -> 31.8 us  [local(): pl.pallas_call(mix_kernel, out_shape=pltpu.VMEM((rows // ways, model), jn...]
where the time goes in v3:
time: 32.7 us; the launch traced here: 32.6 us
  Pallas kernels  31.8 us (97%)
  local copies, waits for them, and re-layouts  0.8 us (2%)
    pallas_call x1, Pallas kernels, local(): pl.pallas_call(mix_kernel, out_shape=pltpu.VMEM((rows // ways, model), jn...  31.8 us
    unnamed x1, local copies, waits for them, and re-layouts  0.8 us

profile of v3, /device:TPU:25, one launch (start us, length us, event | category | flops | bytes accessed | tf_op | source)
XLA Modules:
  0.0 32.6 jit_solution(14775162866580017792)
XLA Ops:
  0.0 31.8 %shard_map.145 = bf16[128,2048]{1,0:T(8,128)(2,1)S(1)} custom-call(f32[16,1]{1,0:T(8,128)} %constant.3.inv_in, bf16[256,1024]{1,0:T(8,128)(2,1)} %tok_in.1, bf16[2048,128]{1,0:T(8,128)(2,1)} %ldown_in.1, bf16[32,2048]{1,0:T(8,128)(2,1)} %bitcast.3, bf16[2048,256]{1,0:T(8,128)(2,1)} %qdown_in.1, bf16[256,1024]{1,0:T(8,128)(2,1)} %up_in.1, ...), custom_call_target="tpu_custom_call" | custom-call | tf_op jit(solution)/shard_map/pallas_call | solution.py:529
  31.8 0.8 %copy.17 = bf16[128,2048]{1,0:T(8,128)(2,1)} copy(bf16[128,2048]{1,0:T(8,128)(2,1)S(1)} %shard_map.145) | data formatting | bytes 1048576

commit v4 on v3

--- a/solution.py
+++ b/solution.py
@@ -28,17 +28,17 @@
     return lax.dot_general(a, b, (dims, ((), ())), preferred_element_type=jnp.float32)
 
 
-def unit(lat_parts, rot_parts, qx_ref, wk_ref, wvt_ref, keys, turned, scores, weights, best_ref, acc_ref, masked):
-    heads, _, rows = qx_ref.shape
+def unit(lat_parts, rot_parts, qx_ref, wk_ref, wvt_ref, keys, turned, scores, weights, best_ref, acc_ref, masked, low, heads):
     latent = jnp.concatenate(lat_parts, 0)
     rot = jnp.concatenate(rot_parts, 0)
     span = latent.shape[0]
-    keys[:span] = dot(latent, wk_ref[...]).astype(jnp.bfloat16)
-    flat = dot(wvt_ref[...], latent, ((1,), (1,))).astype(jnp.bfloat16)
+    lanes = slice(low * NOPE, (low + heads) * NOPE)
+    keys[:span, lanes] = dot(latent, wk_ref[:, lanes]).astype(jnp.bfloat16)
+    flat = dot(wvt_ref[low * VDIM : (low + heads) * VDIM], latent, ((1,), (1,))).astype(jnp.bfloat16)
     for h in range(heads):
-        turned[h, :VDIM, :span] = flat[h * VDIM : (h + 1) * VDIM]
+        turned[low + h, :VDIM, :span] = flat[h * VDIM : (h + 1) * VDIM]
     ring = scores.shape[0]
-    tops = [None] * heads
+    tops = {}
 
     def score(h):
         pair = h // 2 * 2 * NOPE
@@ -67,11 +67,11 @@
 
     for step in range(heads + 2 * LAG):
         if step < heads:
-            score(step)
+            score(low + step)
         if 0 <= step - LAG < heads:
-            soften(step - LAG)
+            soften(low + step - LAG)
         if 0 <= step - 2 * LAG < heads:
-            gather(step - 2 * LAG)
+            gather(low + step - 2 * LAG)
 
 
 def mix_kernel(
@@ -79,8 +79,8 @@
     out_ref,
     inv_ref, tok, ldown, rdown, qdown, up_ref, inner_w, signal_w, lgain_ref, qgain_ref, qup, taps_ref, outer_w, cproj_ref, aproj_ref,
     xbuf, raw_lat, raw_query, edge, rim, padded, conv_ref, wk_ref, wvt_ref, qx_ref,
-    kv, keys, turned, scores, weights, best_ref, acc_ref, att, small, held, cpart, part_buf, in_buf,
-    load_sem, front_send, front_recv, up_send, side_send, kv_recv, share_send, share_recv, tail_send, tail_recv,
+    kv, keys, turned, scores, weights, best_ref, acc_ref, att, small, held, cpart, part_buf, in_buf, far_query, far_qx, far_best, far_acc, back, back_top,
+    load_sem, front_send, front_recv, up_send, side_send, kv_recv, share_send, share_recv, tail_send, tail_recv, far_sem, back_send, back_recv,
 ):
     me = lax.axis_index("sp")
     t = lax.axis_index("tp")
@@ -92,6 +92,10 @@
     b1 = (me // 2) % 2
     heads, _, rows = qx_ref.shape
     short = rows // ways
+    span = 4 * (planes - 1)
+    helper = z == 0
+    helped = z == planes - 1
+    deep = lax.select(helped, z - 1, z)
     cross = (1 - 2 * b0, 2 - 4 * b1, 3 - 2 * b0 - 4 * b1)
     after = lax.rem(me + 1, total)
     before = lax.rem(me + total - 1, total)
@@ -128,17 +132,22 @@
     for copy in token_sends:
         copy.start()
     loads[4].wait()
-    position = (me * rows + lax.broadcasted_iota(jnp.int32, (1, rows), 1)).astype(jnp.float32)
-    angle = inv_ref[...] * position
-    cosine = jnp.cos(angle)
-    sine = jnp.sin(angle)
     half = ROPE // 2
 
-    def rotated(values):
-        a = values[:half]
-        b = values[half:]
-        return jnp.concatenate([a * cosine - b * sine, a * sine + b * cosine], 0).astype(jnp.bfloat16)
-
+    def turner(rank):
+        position = (rank * rows + lax.broadcasted_iota(jnp.int32, (1, rows), 1)).astype(jnp.float32)
+        angle = inv_ref[...] * position
+        cosine = jnp.cos(angle)
+        sine = jnp.sin(angle)
+
+        def rotated(values):
+            a = values[:half]
+            b = values[half:]
+            return jnp.concatenate([a * cosine - b * sine, a * sine + b * cosine], 0).astype(jnp.bfloat16)
+
+        return rotated
+
+    rotated = turner(me)
     for h in range(heads):
         turned[h, VDIM:] = jnp.ones((ONES, turned.shape[2]), jnp.bfloat16)
     depth = tok.shape[1]
@@ -179,6 +188,15 @@
     raw_query[ways - 1] = rest(small[:, spots[1]], qdown).astype(jnp.bfloat16)
     for copy in query_sends:
         copy.start()
+    ask = pltpu.make_async_remote_copy(
+        raw_query.at[ways - 1], far_query.at[ways - 1], far_sem.at[0], far_sem.at[1],
+        device_id=(lax.rem(me + 4, total), t), device_id_type=MESH,
+    )
+
+    @pl.when(helped)
+    def _():
+        ask.start()
+
     turn_part = rest(small[:, spots[2].start : spots[2].start + ROPE], rdown)
     turn = jnp.concatenate([turn_part, jnp.zeros((rows, LANES - ROPE), jnp.float32)], 1).T
     spun = rotated(turn[:ROPE])
@@ -232,7 +250,7 @@
         for step in steps:
             starts = d % 4 == 0 if step > 1 else jnp.logical_or(d % 4 == 0, d % 4 == 3)
 
-            @pl.when(jnp.logical_and(starts, z + step < planes))
+            @pl.when(jnp.logical_and(starts, z + step < planes - (z == d).astype(jnp.int32)))
             def _():
                 go(send(me - 4 * d, me + 4 * step, up_send.at[d, step - 1]))
 
@@ -257,7 +275,7 @@
     def own_side(go, ks):
         for k in ks:
 
-            @pl.when((b0, b1, b1)[k] == 0)
+            @pl.when(jnp.logical_or((b0, b1, b1)[k] == 0, helper))
             def _():
                 go(send(me, me + cross[k], side_send.at[0, k]))
 
@@ -277,18 +295,21 @@
     loads[10].wait()
     for copy in query_sends:
         copy.wait_recv()
-    scale = (NOPE + ROPE) ** (-0.5) * log2e
-    query = (dot(whole(raw_query, qgain_ref), qup[...]) * scale).T
-    size = NOPE + ROPE
-    for h in range(heads):
-        base = h * size
-        side = h % 2 * NOPE
-        qx_ref[h, side : side + NOPE] = query[base : base + NOPE].astype(jnp.bfloat16)
-        qx_ref[h, NOPE - side : 2 * NOPE - side] = jnp.zeros((NOPE, rows), jnp.bfloat16)
-        qx_ref[h, 2 * NOPE : 2 * NOPE + ROPE] = rotated(query[base + NOPE : base + size])
-        qx_ref[h, 2 * NOPE + ROPE :] = jnp.zeros((LANES - ROPE, rows), jnp.bfloat16)
-
-    def run(blocks, masked):
+    def prepare(raw, spin, queries):
+        scale = (NOPE + ROPE) ** (-0.5) * log2e
+        query = (dot(whole(raw, qgain_ref), qup[...]) * scale).T
+        size = NOPE + ROPE
+        for h in range(heads):
+            base = h * size
+            side = h % 2 * NOPE
+            queries[h, side : side + NOPE] = query[base : base + NOPE].astype(jnp.bfloat16)
+            queries[h, NOPE - side : 2 * NOPE - side] = jnp.zeros((NOPE, rows), jnp.bfloat16)
+            queries[h, 2 * NOPE : 2 * NOPE + ROPE] = spin(query[base + NOPE : base + size])
+            queries[h, 2 * NOPE + ROPE :] = jnp.zeros((LANES - ROPE, rows), jnp.bfloat16)
+
+    prepare(raw_query, rotated, qx_ref)
+
+    def run(blocks, masked, queries=qx_ref, best=best_ref, acc=acc_ref, low=0, count=heads):
         lat_parts = []
         rot_parts = []
         for j in blocks:
@@ -297,7 +318,7 @@
             spin = jnp.concatenate([spin, jnp.zeros((LANES - ROPE, rows), jnp.float32)], 0)
             rot_parts.append(spin.T.astype(jnp.bfloat16))
         unit(
-            lat_parts, rot_parts, qx_ref, wk_ref, wvt_ref, keys, turned, scores, weights, best_ref, acc_ref, masked
+            lat_parts, rot_parts, queries, wk_ref, wvt_ref, keys, turned, scores, weights, best, acc, masked, low, count
         )
 
     lift(0, begin, (2,))
@@ -319,25 +340,71 @@
     def _():
         rim_copy.start()
 
-    @pl.when(z > 0)
+    @pl.when(deep > 0)
     def _():
         relay(1, (0, 1))
 
     loads[12].wait()
     held[...] = rest(project(tok[...], outer_w, 0), outer_w)
 
-    @pl.when(z > 0)
+    @pl.when(deep > 0)
     def _():
         pass_on(1, (2,))
 
 
-    @pl.when(b0 == 1)
+    far_shares = to_mates(far_query.at[ways - 1], far_query, 4)
+    groups, members = back_top.shape[:2]
+
+    def returns(g):
+        return [
+            pltpu.make_async_remote_copy(
+                buf.at[g], buf.at[g], back_send.at[g, i], back_recv.at[g, i],
+                device_id=(lax.rem(me + span, total), t), device_id_type=MESH,
+            )
+            for i, buf in enumerate((back, back_top))
+        ]
+
+    @pl.when(helper)
+    def _():
+        ask.wait_recv()
+        for copy in far_shares:
+            copy.start()
+        for c in cross:
+            collect(me + c)
+        for copy in far_shares:
+            copy.wait_recv()
+        prepare(far_query, turner(me + span), far_qx)
+        far_best[...] = jnp.full(far_best.shape, neg_fill, jnp.float32)
+        far_acc[...] = jnp.zeros(far_acc.shape, jnp.float32)
+        base = me - me % 4
+        for c in cross:
+            landed(me + c)
+        for g in range(groups):
+
+            @pl.loop(0, 2)
+            def _(p):
+                run([base + 2 * p, base + 2 * p + 1], False, far_qx, far_best, far_acc, g * members, members)
+
+            for i in range(members):
+                acc = far_acc[g * members + i]
+                mass = acc[VDIM : VDIM + 1]
+                back[g, i] = (acc[:VDIM] * (1.0 / mass)).astype(jnp.bfloat16)
+                back_top[g, i : i + 1] = far_best[g * members + i] + jnp.log2(mass)
+            for copy in returns(g):
+                copy.start()
+
+    lower = jnp.logical_not(helper)
+
+    @pl.when(jnp.logical_and(b0 == 1, lower))
     def _():
         collect(me + cross[0])
         landed(me + cross[0])
+
+    @pl.when(b0 == 1)
+    def _():
         run([me + cross[0]], False)
 
-    @pl.when(b1 == 1)
+    @pl.when(jnp.logical_and(b1 == 1, lower))
     def _():
         collect(me + cross[1])
         collect(me + cross[2])
@@ -364,7 +431,7 @@
         loads[13].wait()
         cpart[...] = dot(conv_ref[...], cproj_ref[...])
 
-    @pl.loop(0, 2 * z + 1)
+    @pl.loop(0, 2 * deep + 1)
     def _(n):
         plane = (n + 1) // 2
         odd = n % 2
@@ -373,11 +440,11 @@
         def ahead(when):
             then = me - 4 * ((n + 2) // 2)
 
-            @pl.when(jnp.logical_and(when, jnp.logical_and(n < 2 * z, odd == 0)))
+            @pl.when(jnp.logical_and(when, jnp.logical_and(n < 2 * deep, odd == 0)))
             def _():
                 collect(then + cross[0])
 
-            @pl.when(jnp.logical_and(when, jnp.logical_and(n < 2 * z, odd == 1)))
+            @pl.when(jnp.logical_and(when, jnp.logical_and(n < 2 * deep, odd == 1)))
             def _():
                 collect(then + cross[1])
                 collect(then + cross[2])
@@ -390,7 +457,7 @@
         ahead(jnp.logical_not(late))
         far = (n + b1) // 2 + 2
 
-        @pl.when(jnp.logical_and(jnp.logical_or(n == 0, (n + b1) % 2 == 0), far <= z))
+        @pl.when(jnp.logical_and(jnp.logical_or(n == 0, (n + b1) % 2 == 0), far <= deep))
         def _():
             relay(far)
 
@@ -401,13 +468,31 @@
         left = own + (1 - odd) * cross[1]
         right = own + odd * cross[0] + (1 - odd) * cross[2]
 
-        @pl.when(n + b1 > 0)
+        @pl.when(jnp.logical_and(n + b1 > 0, lower))
         def _():
             landed(left)
             landed(right)
+
+        @pl.when(n + b1 > 0)
+        def _():
             run([left, right], False)
 
         ahead(late)
+
+    @pl.when(helped)
+    def _():
+        for g in range(groups):
+            for copy in returns(g):
+                copy.wait_recv()
+            for i in range(members):
+                h = g * members + i
+                mine = best_ref[h]
+                other = back_top[g, i : i + 1]
+                top = jnp.maximum(mine, other)
+                keep = jnp.exp2(mine - top)
+                add = jnp.exp2(other - top)
+                acc_ref[h, :VDIM] = acc_ref[h, :VDIM] * keep + back[g, i].astype(jnp.float32) * add
+                acc_ref[h, VDIM:] = acc_ref[h, VDIM:] * keep + add
 
     loads[14].wait()
 
@@ -415,7 +500,7 @@
         flat = []
         for h in range(heads):
             acc = acc_ref[h, :, at]
-            flat.append(acc[:VDIM] / acc[VDIM : VDIM + 1])
+            flat.append(acc[:VDIM] * (1.0 / acc[VDIM : VDIM + 1]))
         return jnp.concatenate(flat, 0).T.astype(jnp.bfloat16)
 
     if short % LANES:
@@ -465,17 +550,29 @@
     lift(0, finish, (1, 2, 3))
     own_side(finish, (0, 1, 2))
 
-    @pl.when(b0 == 1)
+    @pl.when(helped)
+    def _():
+        ask.wait_send()
+
+    @pl.when(helper)
+    def _():
+        for copy in far_shares:
+            copy.wait_send()
+        for g in range(groups):
+            for copy in returns(g):
+                copy.wait_send()
+
+    @pl.when(jnp.logical_or(b0 == 1, helper))
     def _():
         for copy in shares(me + cross[0]):
             copy.wait_send()
 
-    @pl.when(b1 == 1)
+    @pl.when(jnp.logical_or(b1 == 1, helper))
     def _():
         for copy in shares(me + cross[1]) + shares(me + cross[2]):
             copy.wait_send()
 
-    @pl.loop(1, z + 1)
+    @pl.loop(1, deep + 1)
     def _(d):
         j = me - 4 * d
         lift(d, finish, (1, 2, 3))
@@ -515,6 +612,7 @@
     dma = pltpu.SemaphoreType.DMA
     mates = ways - 1
     ring = min(heads, RING)
+    groups = 1 if heads % 4 else 2
     big = (
         inverse[:, None], tokens, latent_down, rotary_down.T, query_down, latent_up, inner_gate, conv_input,
         latent_gain[None, :], query_gain[None, :], query_up, conv_taps, outer_gate, conv_project, attend_project,
@@ -556,9 +654,15 @@
             full_type(rows, model),
             half_type(mates, rows // ways, model),
             half_type(mates, rows // ways, model),
+            half_type(ways, rows, query_down.shape[1]),
+            half_type(heads, 2 * NOPE + LANES, rows),
+            full_type(heads, 1, rows),
+            full_type(heads, VDIM + ONES, rows),
+            half_type(groups, heads // groups, VDIM, rows),
+            full_type(groups, heads // groups, rows),
             dma((len(big),)),
-            dma((4, mates)),
-            dma((4, mates)),
+            dma((5, mates)),
+            dma((5, mates)),
             dma((blocks // 4, 3)),
             dma((blocks // 4, 3)),
             dma((blocks,)),
@@ -566,6 +670,9 @@
             dma((blocks, mates)),
             dma((mates, CHUNKS)),
             dma((mates, CHUNKS)),
+            dma((2,)),
+            dma((groups, 2)),
+            dma((groups, 2)),
         ],
         compiler_params=pltpu.CompilerParams(
             vmem_limit_bytes=60 * 1024 * 1024, collective_id=0, has_side_effects=True

time: 32.7 us -> 28.6 us (0.87)
  Pallas kernels: 31.8 us -> 27.5 us
    pallas_call x1, Pallas kernels: 31.8 us -> 27.5 us  [local(): pl.pallas_call(mix_kernel, out_shape=pltpu.VMEM((rows // ways, model), jn...]
where the time goes in v4:
time: 28.6 us; the launch traced here: 28.3 us
  Pallas kernels  27.5 us (96%)
  local copies, waits for them, and re-layouts  0.8 us (3%)
    pallas_call x1, Pallas kernels, local(): pl.pallas_call(mix_kernel, out_shape=pltpu.VMEM((rows // ways, model), jn...  27.5 us
    unnamed x1, local copies, waits for them, and re-layouts  0.8 us

profile of v4, /device:TPU:25, one launch (start us, length us, event | category | flops | bytes accessed | tf_op | source)
XLA Modules:
  0.0 28.3 jit_solution(18304976591097800676)
XLA Ops:
  0.0 27.5 %shard_map.145 = bf16[128,2048]{1,0:T(8,128)(2,1)S(1)} custom-call(f32[16,1]{1,0:T(8,128)} %constant.3.inv_in, bf16[256,1024]{1,0:T(8,128)(2,1)} %tok_in.1, bf16[2048,128]{1,0:T(8,128)(2,1)} %ldown_in.1, bf16[32,2048]{1,0:T(8,128)(2,1)} %bitcast.3, bf16[2048,256]{1,0:T(8,128)(2,1)} %qdown_in.1, bf16[256,1024]{1,0:T(8,128)(2,1)} %up_in.1, ...), custom_call_target="tpu_custom_call" | custom-call | tf_op jit(solution)/shard_map/pallas_call | solution.py:627
  27.5 0.8 %copy.17 = bf16[128,2048]{1,0:T(8,128)(2,1)} copy(bf16[128,2048]{1,0:T(8,128)(2,1)S(1)} %shard_map.145) | data formatting | bytes 1048576

commit v5 on v4

--- a/solution.py
+++ b/solution.py
@@ -16,6 +16,7 @@
 LAG = 2
 EAGER = 9
 CHUNKS = 2
+TAG = 16
 
 MESH = pl.DeviceIdType.MESH
 neg_fill = -1e30
@@ -28,13 +29,16 @@
     return lax.dot_general(a, b, (dims, ((), ())), preferred_element_type=jnp.float32)
 
 
-def unit(lat_parts, rot_parts, qx_ref, wk_ref, wvt_ref, keys, turned, scores, weights, best_ref, acc_ref, masked, low, heads):
+def unit(lat_parts, rot_parts, factors, qx_ref, wk_ref, wvt_ref, keys, turned, scores, weights, best_ref, acc_ref, masked, low, heads):
     latent = jnp.concatenate(lat_parts, 0)
     rot = jnp.concatenate(rot_parts, 0)
     span = latent.shape[0]
     lanes = slice(low * NOPE, (low + heads) * NOPE)
-    keys[:span, lanes] = dot(latent, wk_ref[:, lanes]).astype(jnp.bfloat16)
-    flat = dot(wvt_ref[low * VDIM : (low + heads) * VDIM], latent, ((1,), (1,))).astype(jnp.bfloat16)
+    down = jnp.concatenate([f[0] for f in factors], 0)
+    along = jnp.concatenate([f[1] for f in factors], 1)
+    keys[:span, lanes] = (dot(latent, wk_ref[:, lanes]) * down).astype(jnp.bfloat16)
+    flat = dot(wvt_ref[low * VDIM : (low + heads) * VDIM], latent, ((1,), (1,)))
+    flat = (flat * along).astype(jnp.bfloat16)
     for h in range(heads):
         turned[low + h, :VDIM, :span] = flat[h * VDIM : (h + 1) * VDIM]
     ring = scores.shape[0]
@@ -78,7 +82,7 @@
     inv_in, tok_in, ldown_in, rdown_in, qdown_in, up_in, inner_in, signal_in, lgain_in, qgain_in, qup_in, taps_in, outer_in, cproj_in, aproj_in,
     out_ref,
     inv_ref, tok, ldown, rdown, qdown, up_ref, inner_w, signal_w, lgain_ref, qgain_ref, qup, taps_ref, outer_w, cproj_ref, aproj_ref,
-    xbuf, raw_lat, raw_query, edge, rim, padded, conv_ref, wk_ref, wvt_ref, qx_ref,
+    xbuf, comb, raw_query, edge, rim, padded, conv_ref, wk_ref, wvt_ref, qx_ref,
     kv, keys, turned, scores, weights, best_ref, acc_ref, att, small, held, cpart, part_buf, in_buf, far_query, far_qx, far_best, far_acc, back, back_top,
     load_sem, front_send, front_recv, up_send, side_send, kv_recv, share_send, share_recv, tail_send, tail_recv, far_sem, back_send, back_recv,
 ):
@@ -103,9 +107,19 @@
 
     barrier = pltpu.get_barrier_semaphore()
     targets = [(me, mate) for mate in mates] + [(me + c, t) for c in cross]
-    targets += [(lax.rem(me + 4 * d, total), t) for d in range(1, planes)] + [(after, t), (before, t)]
+    targets += [(lax.rem(me + 4 * d, total), t) for d in range(1, planes)]
     for target in targets:
         pl.semaphore_signal(barrier, inc=1, device_id=target, device_id_type=MESH)
+
+    @pl.when(me > 0)
+    def _():
+        pl.semaphore_signal(barrier, inc=1, device_id=(before, t), device_id_type=MESH)
+
+    @pl.when(me + 1 < total)
+    def _():
+        pl.semaphore_signal(barrier, inc=1, device_id=(after, t), device_id_type=MESH)
+
+    ends = (me == 0).astype(jnp.int32) + (me + 1 == total).astype(jnp.int32)
 
     pairs = (
         (tok_in, tok), (ldown_in, ldown), (rdown_in, rdown), (qdown_in, qdown), (inv_in, inv_ref),
@@ -116,7 +130,7 @@
     for copy in loads[:EAGER]:
         copy.start()
 
-    pl.semaphore_wait(barrier, len(targets))
+    pl.semaphore_wait(barrier, len(targets) + 2 - ends)
     loads[0].wait()
 
     def to_mates(source, slots, kind):
@@ -154,12 +168,10 @@
 
     def rows_from(weight, o):
         at = pl.multiple_of(lax.rem(t + ways - o, ways) * depth, depth)
-        if weight is rdown:
-            return weight[:, pl.ds(at, depth)]
         return weight[pl.ds(at, depth), :]
 
     def project(x, weight, o):
-        return dot(x, rows_from(weight, o), ((1,), (1 if weight is rdown else 0,)))
+        return dot(x, rows_from(weight, o))
 
     def rest(value, weight):
         more = project(xbuf[0], weight, 1)
@@ -171,50 +183,43 @@
         copy.wait()
     for copy in loads[EAGER:]:
         copy.start()
-    narrow = (ldown, qdown, rdown)
-    spots = []
-    for weight in narrow:
-        start = spots[-1].stop if spots else 0
-        spots.append(slice(start, start + (LANES if weight is rdown else weight.shape[1])))
-    for weight, spot in zip(narrow, spots):
-        small[:, spot.start : spot.start + (ROPE if weight is rdown else weight.shape[1])] = project(tok[...], weight, 0)
+    wide = kv.shape[3]
+    if wide < LANES:
+        comb[:, :LANES] = jnp.zeros((comb.shape[0], LANES), jnp.bfloat16)
+    comb[:, :wide] = ldown[...]
+    tall = jnp.concatenate([rdown[...].astype(jnp.float32), jnp.zeros((LANES - ROPE, comb.shape[0]), jnp.float32)], 0)
+    comb[:, LANES:] = tall.T.astype(jnp.bfloat16)
+    small[:, : 2 * LANES] = project(tok[...], comb, 0)
+    small[:, 2 * LANES :] = project(tok[...], qdown, 0)
     for copy in token_sends:
         copy.wait_recv()
-    raw_lat[ways - 1] = rest(small[:, spots[0]], ldown).astype(jnp.bfloat16)
-    latent_sends = to_mates(raw_lat.at[ways - 1], raw_lat, 1)
-    query_sends = to_mates(raw_query.at[ways - 1], raw_query, 2)
-    for copy in latent_sends:
-        copy.start()
-    raw_query[ways - 1] = rest(small[:, spots[1]], qdown).astype(jnp.bfloat16)
-    for copy in query_sends:
-        copy.start()
-    ask = pltpu.make_async_remote_copy(
-        raw_query.at[ways - 1], far_query.at[ways - 1], far_sem.at[0], far_sem.at[1],
-        device_id=(lax.rem(me + 4, total), t), device_id_type=MESH,
-    )
-
-    @pl.when(helped)
-    def _():
-        ask.start()
-
-    turn_part = rest(small[:, spots[2].start : spots[2].start + ROPE], rdown)
-    turn = jnp.concatenate([turn_part, jnp.zeros((rows, LANES - ROPE), jnp.float32)], 1).T
+    both = rest(small[:, : 2 * LANES], comb)
+    raw_query[ways - 1] = rest(small[:, 2 * LANES :], qdown).astype(jnp.bfloat16)
+    piece = both[:, :wide].astype(jnp.bfloat16)
+    kv[me, t, :rows] = piece
+    mass = piece.astype(jnp.float32)
+    mass = jnp.sum(mass * mass, -1, keepdims=True)
+    lane = lax.broadcasted_iota(jnp.int32, (1, LANES), 1)
+    turn = jnp.where(lane == ROPE, mass, both[:, LANES:]).T
     spun = rotated(turn[:ROPE])
-
+    for s in range(ways):
+
+        @pl.when(t == s)
+        def _():
+            kv[me, s, rows : rows + ROPE] = spun[:, s * wide : (s + 1) * wide]
+
+    mass = turn[ROPE : ROPE + 1]
+    high = mass.astype(jnp.bfloat16).astype(jnp.float32)
+    folds = rows // wide
+    tags = [part[:, r * wide : (r + 1) * wide] for part in (high, mass - high) for r in range(folds)]
+    if len(tags) < TAG:
+        tags.append(jnp.zeros((TAG - len(tags), wide), jnp.float32))
+    kv[me, t, rows + ROPE :] = jnp.concatenate(tags, 0).astype(jnp.bfloat16)
 
     def whole(raw, gain_ref):
         values = jnp.concatenate([raw[lax.rem(t + ways - 1 - s, ways)] for s in range(ways)], 1).astype(jnp.float32)
         factor = lax.rsqrt(jnp.mean(values * values, -1, keepdims=True) + norm_epsilon)
         return (values * factor * gain_ref[...]).astype(jnp.bfloat16)
-
-    for copy in latent_sends:
-        copy.wait_recv()
-    loads[5].wait()
-    latent_norm = whole(raw_lat, lgain_ref)
-    wide = kv.shape[3]
-    for s in range(ways):
-        kv[me, s, :rows] = latent_norm[:, s * wide : (s + 1) * wide]
-        kv[me, s, rows:] = spun[:, s * wide : (s + 1) * wide]
 
     def send(j, target, sem):
         return pltpu.make_async_remote_copy(
@@ -279,14 +284,45 @@
             def _():
                 go(send(me, me + cross[k], side_send.at[0, k]))
 
+    query_sends = to_mates(raw_query.at[ways - 1], raw_query, 2)
+    for copy in query_sends:
+        copy.start()
+    ask = pltpu.make_async_remote_copy(
+        raw_query.at[ways - 1], far_query.at[ways - 1], far_sem.at[0], far_sem.at[1],
+        device_id=(lax.rem(me + 4, total), t), device_id_type=MESH,
+    )
+
+    @pl.when(helped)
+    def _():
+        ask.start()
+
     lift(0, begin, (1,))
     own_side(begin, (0, 1))
+    for copy in shares(me):
+        copy.start()
+    loads[8].wait()
+    inner = rest(project(tok[...], inner_w, 0), inner_w)
+    loads[11].wait()
+    signal = rest(project(tok[...], signal_w, 0), signal_w)
+    gated = (inner * signal).astype(jnp.bfloat16)
+    padded[EDGE:] = gated.astype(jnp.float32)
+    edge[...] = gated[rows - EDGE :]
+    rim_copy = pltpu.make_async_remote_copy(
+        edge, rim, front_send.at[3, 0], front_recv.at[3, 0], device_id=(after, t), device_id_type=MESH
+    )
+
+    @pl.when(me + 1 < total)
+    def _():
+        rim_copy.start()
+
+    loads[5].wait()
     loads[9].wait()
     low = lax.broadcasted_iota(jnp.int32, (1, 2 * NOPE), 1) < NOPE
     width = NOPE + VDIM
+    gain = jnp.concatenate([lgain_ref[...], jnp.zeros((LANES - 1, lgain_ref.shape[1]), jnp.float32)], 0).T[:, :1]
     for p in range(heads // 2):
-        even = up_ref[:, 2 * p * width : (2 * p + 1) * width].astype(jnp.float32)
-        odd = up_ref[:, (2 * p + 1) * width : (2 * p + 2) * width].astype(jnp.float32)
+        even = up_ref[:, 2 * p * width : (2 * p + 1) * width].astype(jnp.float32) * gain
+        odd = up_ref[:, (2 * p + 1) * width : (2 * p + 2) * width].astype(jnp.float32) * gain
         at = slice(p * width, (p + 1) * width)
         wk_ref[:, at] = jnp.where(low, even, pltpu.roll(odd, NOPE, 1)).astype(jnp.bfloat16)
         wvt_ref[at] = jnp.where(low, pltpu.roll(even, NOPE, 1), odd).T.astype(jnp.bfloat16)
@@ -312,53 +348,49 @@
     def run(blocks, masked, queries=qx_ref, best=best_ref, acc=acc_ref, low=0, count=heads):
         lat_parts = []
         rot_parts = []
+        factors = []
         for j in blocks:
             lat_parts.append(jnp.concatenate([kv[j, s, :rows] for s in range(ways)], 1))
-            spin = jnp.concatenate([kv[j, s, rows:] for s in range(ways)], 1).astype(jnp.float32)
-            spin = jnp.concatenate([spin, jnp.zeros((LANES - ROPE, rows), jnp.float32)], 0)
-            rot_parts.append(spin.T.astype(jnp.bfloat16))
+            spin = jnp.concatenate([kv[j, s, rows : rows + ROPE] for s in range(ways)], 1).astype(jnp.float32)
+            tag = kv[j, 0, rows + ROPE :].astype(jnp.float32)
+            for s in range(1, ways):
+                tag = tag + kv[j, s, rows + ROPE :].astype(jnp.float32)
+            mass = jnp.concatenate([tag[r : r + 1] + tag[folds + r : folds + r + 1] for r in range(folds)], 1)
+            along = lax.rsqrt(mass * (1.0 / (ways * wide)) + norm_epsilon)
+            spin = jnp.concatenate([spin, along, jnp.zeros((LANES - ROPE - 1, rows), jnp.float32)], 0).T
+            rot_parts.append(spin.astype(jnp.bfloat16))
+            factors.append((spin[:, ROPE : ROPE + 1], along))
         unit(
-            lat_parts, rot_parts, queries, wk_ref, wvt_ref, keys, turned, scores, weights, best, acc, masked, low, count
+            lat_parts, rot_parts, factors, queries, wk_ref, wvt_ref, keys, turned, scores, weights, best, acc, masked, low, count
         )
 
     lift(0, begin, (2,))
     own_side(begin, (2,))
+    loads[12].wait()
+    held[...] = rest(project(tok[...], outer_w, 0), outer_w)
+
+    @pl.when(deep > 0)
+    def _():
+        relay(1, (0, 1))
+
+
+    landed(me)
     run([me], True)
     lift(0, begin, (3,))
-    loads[8].wait()
-    inner = rest(project(tok[...], inner_w, 0), inner_w)
-    loads[11].wait()
-    signal = rest(project(tok[...], signal_w, 0), signal_w)
-    gated = (inner * signal).astype(jnp.bfloat16)
-    padded[EDGE:] = gated.astype(jnp.float32)
-    edge[...] = gated[rows - EDGE :]
-    rim_copy = pltpu.make_async_remote_copy(
-        edge, rim, front_send.at[3, 0], front_recv.at[3, 0], device_id=(after, t), device_id_type=MESH
-    )
-
-    @pl.when(me + 1 < total)
-    def _():
-        rim_copy.start()
 
     @pl.when(deep > 0)
     def _():
-        relay(1, (0, 1))
-
-    loads[12].wait()
-    held[...] = rest(project(tok[...], outer_w, 0), outer_w)
-
-    @pl.when(deep > 0)
-    def _():
         pass_on(1, (2,))
 
 
     far_shares = to_mates(far_query.at[ways - 1], far_query, 4)
-    groups, members = back_top.shape[:2]
+    groups = back_send.shape[0]
+    bounds = [(g * heads // groups, heads // groups) for g in range(groups)]
 
     def returns(g):
         return [
             pltpu.make_async_remote_copy(
-                buf.at[g], buf.at[g], back_send.at[g, i], back_recv.at[g, i],
+                buf.at[pl.ds(*bounds[g])], buf.at[pl.ds(*bounds[g])], back_send.at[g, i], back_recv.at[g, i],
                 device_id=(lax.rem(me + span, total), t), device_id_type=MESH,
             )
             for i, buf in enumerate((back, back_top))
@@ -369,40 +401,54 @@
         ask.wait_recv()
         for copy in far_shares:
             copy.start()
+        far_best[...] = jnp.full(far_best.shape, neg_fill, jnp.float32)
+        far_acc[...] = jnp.zeros(far_acc.shape, jnp.float32)
         for c in cross:
             collect(me + c)
         for copy in far_shares:
             copy.wait_recv()
         prepare(far_query, turner(me + span), far_qx)
-        far_best[...] = jnp.full(far_best.shape, neg_fill, jnp.float32)
-        far_acc[...] = jnp.zeros(far_acc.shape, jnp.float32)
-        base = me - me % 4
-        for c in cross:
-            landed(me + c)
+        landed(me + cross[0])
         for g in range(groups):
 
             @pl.loop(0, 2)
             def _(p):
-                run([base + 2 * p, base + 2 * p + 1], False, far_qx, far_best, far_acc, g * members, members)
-
-            for i in range(members):
-                acc = far_acc[g * members + i]
+                if g == 0:
+
+                    @pl.when(p == 1)
+                    def _():
+                        landed(me + cross[1])
+                        landed(me + cross[2])
+
+                first = me + p * cross[1]
+                then = me + (1 - p) * cross[0] + p * cross[2]
+                run([first, then], False, far_qx, far_best, far_acc, *bounds[g])
+
+            for h in range(bounds[g][0], sum(bounds[g])):
+                acc = far_acc[h]
                 mass = acc[VDIM : VDIM + 1]
-                back[g, i] = (acc[:VDIM] * (1.0 / mass)).astype(jnp.bfloat16)
-                back_top[g, i : i + 1] = far_best[g * members + i] + jnp.log2(mass)
+                back[h] = (acc[:VDIM] * (1.0 / mass)).astype(jnp.bfloat16)
+                back_top[h] = far_best[h] + jnp.log2(mass)
             for copy in returns(g):
                 copy.start()
 
     lower = jnp.logical_not(helper)
+    corner = jnp.logical_and(b0 + b1 == 0, deep > 0)
 
     @pl.when(jnp.logical_and(b0 == 1, lower))
     def _():
         collect(me + cross[0])
         landed(me + cross[0])
 
-    @pl.when(b0 == 1)
-    def _():
-        run([me + cross[0]], False)
+    alone = lax.select(corner, me - 4, me + cross[0])
+
+    @pl.when(corner)
+    def _():
+        landed(alone)
+
+    @pl.when(jnp.logical_or(b0 == 1, corner))
+    def _():
+        run([alone], False)
 
     @pl.when(jnp.logical_and(b1 == 1, lower))
     def _():
@@ -444,9 +490,12 @@
             def _():
                 collect(then + cross[0])
 
+            @pl.when(jnp.logical_and(when, jnp.logical_and(n < 2 * deep, jnp.logical_xor(odd == 1, corner))))
+            def _():
+                collect(then + cross[1])
+
             @pl.when(jnp.logical_and(when, jnp.logical_and(n < 2 * deep, odd == 1)))
             def _():
-                collect(then + cross[1])
                 collect(then + cross[2])
 
         @pl.when(jnp.logical_and(n == 0, b1 == 1))
@@ -465,33 +514,40 @@
         def _():
             convolve()
 
-        left = own + (1 - odd) * cross[1]
-        right = own + odd * cross[0] + (1 - odd) * cross[2]
-
-        @pl.when(jnp.logical_and(n + b1 > 0, lower))
+        left = lax.select(corner, own + odd * cross[0] + (1 - odd) * cross[2], own + (1 - odd) * cross[1])
+        right = lax.select(
+            corner, own + odd * cross[1] - (1 - odd) * 4, own + odd * cross[0] + (1 - odd) * cross[2]
+        )
+        full = jnp.logical_and(n + b1 > 0, jnp.logical_not(jnp.logical_and(corner, n == 2 * deep)))
+
+        @pl.when(jnp.logical_and(full, lower))
         def _():
             landed(left)
             landed(right)
 
-        @pl.when(n + b1 > 0)
+        @pl.when(full)
         def _():
             run([left, right], False)
 
         ahead(late)
+
+    @pl.when(corner)
+    def _():
+        landed(me - 4 * deep + cross[2])
+        run([me - 4 * deep + cross[2]], False)
 
     @pl.when(helped)
     def _():
         for g in range(groups):
             for copy in returns(g):
                 copy.wait_recv()
-            for i in range(members):
-                h = g * members + i
+            for h in range(bounds[g][0], sum(bounds[g])):
                 mine = best_ref[h]
-                other = back_top[g, i : i + 1]
+                other = back_top[h]
                 top = jnp.maximum(mine, other)
                 keep = jnp.exp2(mine - top)
                 add = jnp.exp2(other - top)
-                acc_ref[h, :VDIM] = acc_ref[h, :VDIM] * keep + back[g, i].astype(jnp.float32) * add
+                acc_ref[h, :VDIM] = acc_ref[h, :VDIM] * keep + back[h].astype(jnp.float32) * add
                 acc_ref[h, VDIM:] = acc_ref[h, VDIM:] * keep + add
 
     loads[14].wait()
@@ -540,7 +596,7 @@
             tails[o * CHUNKS + c].wait_recv()
             result = result + in_buf[o, :, cols].astype(jnp.float32)
         out_ref[:, cols] = result.astype(jnp.bfloat16)
-    for copy in tails + token_sends + latent_sends + query_sends:
+    for copy in tails + token_sends + shares(me) + query_sends:
         copy.wait_send()
 
     @pl.when(me + 1 < total)
@@ -632,7 +688,7 @@
         scratch_shapes=[pltpu.VMEM(array.shape, array.dtype) for array in big]
         + [
             half_type(mates, *tokens.shape),
-            half_type(ways, rows, latent_down.shape[1]),
+            half_type(tokens.shape[1] * ways, 2 * LANES),
             half_type(ways, rows, query_down.shape[1]),
             half_type(EDGE, channels),
             half_type(EDGE, channels),
@@ -641,7 +697,7 @@
             half_type(kvr, heads * NOPE),
             half_type(heads * VDIM, kvr),
             half_type(heads, 2 * NOPE + LANES, rows),
-            half_type(blocks, ways, rows + ROPE, kvr // ways),
+            half_type(blocks, ways, rows + ROPE + TAG, kvr // ways),
             half_type(2 * rows, heads * NOPE),
             half_type(heads, VDIM + ONES, 2 * rows),
             full_type(ring, 2 * rows, rows),
@@ -649,7 +705,7 @@
             full_type(heads, 1, rows),
             full_type(heads, VDIM + ONES, rows),
             half_type(rows, heads * VDIM),
-            full_type(rows, latent_down.shape[1] + query_down.shape[1] + LANES),
+            full_type(rows, 2 * LANES + query_down.shape[1]),
             full_type(rows, channels),
             full_type(rows, model),
             half_type(mates, rows // ways, model),
@@ -658,8 +714,8 @@
             half_type(heads, 2 * NOPE + LANES, rows),
             full_type(heads, 1, rows),
             full_type(heads, VDIM + ONES, rows),
-            half_type(groups, heads // groups, VDIM, rows),
-            full_type(groups, heads // groups, rows),
+            half_type(heads, VDIM, rows),
+            full_type(heads, 1, rows),
             dma((len(big),)),
             dma((5, mates)),
             dma((5, mates)),

time: 28.6 us -> 27.9 us (0.976)
  Pallas kernels: 27.5 us -> 27 us
    pallas_call x1, Pallas kernels: 27.5 us -> 27 us  [local(): pl.pallas_call(mix_kernel, out_shape=pltpu.VMEM((rows // ways, model), jn...]
where the time goes in v5:
time: 27.9 us; the launch traced here: 27.8 us
  Pallas kernels  27 us (97%)
  local copies, waits for them, and re-layouts  0.8 us (3%)
    pallas_call x1, Pallas kernels, local(): pl.pallas_call(mix_kernel, out_shape=pltpu.VMEM((rows // ways, model), jn...  27 us
    unnamed x1, local copies, waits for them, and re-layouts  0.8 us

profile of v5, /device:TPU:25, one launch (start us, length us, event | category | flops | bytes accessed | tf_op | source)
XLA Modules:
  0.0 27.8 jit_solution(7111822286143329816)
XLA Ops:
  0.0 27.0 %shard_map.145 = bf16[128,2048]{1,0:T(8,128)(2,1)S(1)} custom-call(f32[16,1]{1,0:T(8,128)} %constant.3.inv_in, bf16[256,1024]{1,0:T(8,128)(2,1)} %tok_in.1, bf16[2048,128]{1,0:T(8,128)(2,1)} %ldown_in.1, bf16[32,2048]{1,0:T(8,128)(2,1)} %bitcast.3, bf16[2048,256]{1,0:T(8,128)(2,1)} %qdown_in.1, bf16[256,1024]{1,0:T(8,128)(2,1)} %up_in.1, ...), custom_call_target="tpu_custom_call" | custom-call | tf_op jit(solution)/shard_map/pallas_call | solution.py:683
  27.0 0.8 %copy.17 = bf16[128,2048]{1,0:T(8,128)(2,1)} copy(bf16[128,2048]{1,0:T(8,128)(2,1)S(1)} %shard_map.145) | data formatting | bytes 1048576

commit v6 on v5

--- a/solution.py
+++ b/solution.py
@@ -257,7 +257,7 @@
 
             @pl.when(jnp.logical_and(starts, z + step < planes - (z == d).astype(jnp.int32)))
             def _():
-                go(send(me - 4 * d, me + 4 * step, up_send.at[d, step - 1]))
+                go(send(me - 4 * d, me + 4 * step, up_send.at[d // 4 * 2 + d % 4 // 3, step - 1]))
 
     def pass_on(d, ks):
         for k in ks:
@@ -403,11 +403,12 @@
             copy.start()
         far_best[...] = jnp.full(far_best.shape, neg_fill, jnp.float32)
         far_acc[...] = jnp.zeros(far_acc.shape, jnp.float32)
-        for c in cross:
-            collect(me + c)
+        collect(me + cross[0])
         for copy in far_shares:
             copy.wait_recv()
         prepare(far_query, turner(me + span), far_qx)
+        collect(me + cross[1])
+        collect(me + cross[2])
         landed(me + cross[0])
         for g in range(groups):
 
@@ -433,7 +434,7 @@
                 copy.start()
 
     lower = jnp.logical_not(helper)
-    corner = jnp.logical_and(b0 + b1 == 0, deep > 0)
+    corner = jnp.logical_and(b0 == 0, deep > 0)
 
     @pl.when(jnp.logical_and(b0 == 1, lower))
     def _():
@@ -514,9 +515,10 @@
         def _():
             convolve()
 
-        left = lax.select(corner, own + odd * cross[0] + (1 - odd) * cross[2], own + (1 - odd) * cross[1])
+        turned_order = jnp.logical_and(corner, n > 0)
+        left = lax.select(turned_order, own + odd * cross[0] + (1 - odd) * cross[2], own + (1 - odd) * cross[1])
         right = lax.select(
-            corner, own + odd * cross[1] - (1 - odd) * 4, own + odd * cross[0] + (1 - odd) * cross[2]
+            turned_order, own + odd * cross[1] - (1 - odd) * 4, own + odd * cross[0] + (1 - odd) * cross[2]
         )
         full = jnp.logical_and(n + b1 > 0, jnp.logical_not(jnp.logical_and(corner, n == 2 * deep)))
 
@@ -719,7 +721,7 @@
             dma((len(big),)),
             dma((5, mates)),
             dma((5, mates)),
-            dma((blocks // 4, 3)),
+            dma(((blocks // 4 + 1) // 2, 3)),
             dma((blocks // 4, 3)),
             dma((blocks,)),
             dma((blocks, mates)),

time: 27.9 us -> 27.7 us (level)
  Pallas kernels: 27 us -> 26.7 us
where the time goes in v6:
time: 27.7 us; the launch traced here: 27.5 us
  Pallas kernels  26.7 us (96%)
  local copies, waits for them, and re-layouts  0.8 us (3%)
    pallas_call x1, Pallas kernels, local(): pl.pallas_call(mix_kernel, out_shape=pltpu.VMEM((rows // ways, model), jn...  26.7 us
    unnamed x1, local copies, waits for them, and re-layouts  0.8 us

profile of v6, /device:TPU:25, one launch (start us, length us, event | category | flops | bytes accessed | tf_op | source)
XLA Modules:
  0.0 27.5 jit_solution(4131441449600910757)
XLA Ops:
  0.0 26.7 %shard_map.145 = bf16[128,2048]{1,0:T(8,128)(2,1)S(1)} custom-call(f32[16,1]{1,0:T(8,128)} %constant.3.inv_in, bf16[256,1024]{1,0:T(8,128)(2,1)} %tok_in.1, bf16[2048,128]{1,0:T(8,128)(2,1)} %ldown_in.1, bf16[32,2048]{1,0:T(8,128)(2,1)} %bitcast.3, bf16[2048,256]{1,0:T(8,128)(2,1)} %qdown_in.1, bf16[256,1024]{1,0:T(8,128)(2,1)} %up_in.1, ...), custom_call_target="tpu_custom_call" | custom-call | tf_op jit(solution)/shard_map/pallas_call | solution.py:685
  26.7 0.8 %copy.17 = bf16[128,2048]{1,0:T(8,128)(2,1)} copy(bf16[128,2048]{1,0:T(8,128)(2,1)S(1)} %shard_map.145) | data formatting | bytes 1048576

commit v7 on v6

--- a/solution.py
+++ b/solution.py
@@ -14,8 +14,8 @@
 EDGE = 16
 RING = 8
 LAG = 2
-EAGER = 9
-CHUNKS = 2
+EAGER = 15
+CHUNKS = 4
 TAG = 16
 
 MESH = pl.DeviceIdType.MESH

time: 27.7 us -> 27.7 us (level)
  no operation moved by 1% of the time
where the time goes in v7:
time: 27.7 us; the launch traced here: 27.6 us
  Pallas kernels  26.8 us (97%)
  local copies, waits for them, and re-layouts  0.8 us (3%)
    pallas_call x1, Pallas kernels, local(): pl.pallas_call(mix_kernel, out_shape=pltpu.VMEM((rows // ways, model), jn...  26.8 us
    unnamed x1, local copies, waits for them, and re-layouts  0.8 us

profile of v7, /device:TPU:25, one launch (start us, length us, event | category | flops | bytes accessed | tf_op | source)
XLA Modules:
  0.0 27.6 jit_solution(8582209688697628314)
XLA Ops:
  0.0 26.8 %shard_map.145 = bf16[128,2048]{1,0:T(8,128)(2,1)S(1)} custom-call(f32[16,1]{1,0:T(8,128)} %constant.3.inv_in, bf16[256,1024]{1,0:T(8,128)(2,1)} %tok_in.1, bf16[2048,128]{1,0:T(8,128)(2,1)} %ldown_in.1, bf16[32,2048]{1,0:T(8,128)(2,1)} %bitcast.3, bf16[2048,256]{1,0:T(8,128)(2,1)} %qdown_in.1, bf16[256,1024]{1,0:T(8,128)(2,1)} %up_in.1, ...), custom_call_target="tpu_custom_call" | custom-call | tf_op jit(solution)/shard_map/pallas_call | solution.py:685
  26.8 0.8 %copy.17 = bf16[128,2048]{1,0:T(8,128)(2,1)} copy(bf16[128,2048]{1,0:T(8,128)(2,1)S(1)} %shard_map.145) | data formatting | bytes 1048576
